TPU v7x, 32 devices: a whole 2x2x4 slice. The times are simulated.
32 devices in a mesh: kv: 16 (over z, y, x), tp: 2 (over core).
Axes of the slice: x: 2, y: 2, z: 4, core: 2. Of those that a mesh axis runs over, the one named last changes fastest.
Arguments:
- residual_in: bfloat16 [96, 2048], P('kv', 'tp'), may hold values from -36 to 36
- gain_pre: float32 [2048], P('tp'), may hold values from 0.1 to 1.9
- gate_pre: bfloat16 [2048, 5632], P('tp', 'kv'), may hold values from -0.125 to 0.125
- up_pre: bfloat16 [2048, 5632], P('tp', 'kv'), may hold values from -0.125 to 0.125
- down_pre: bfloat16 [5632, 2048], P('kv', 'tp'), may hold values from -0.078125 to 0.078125
- gain_mix: float32 [2048], replicated, may hold values from 0.1 to 1.9
- query_weight: bfloat16 [2048, 2048], P('kv', 'tp'), may hold values from -0.125 to 0.125
- forget_weight: bfloat16 [2048, 2048], P('kv', 'tp'), may hold values from -0.125 to 0.125
- value_weight: bfloat16 [2048, 2048], P('kv', 'tp'), may hold values from -0.125 to 0.125
- outgate_weight: bfloat16 [2048, 2048], P('kv', 'tp'), may hold values from -0.125 to 0.125
- lower_bound: float32 [2048], P('tp'), may hold values from 0.05 to 0.95
- head_gain: float32 [2048], P('tp'), may hold values from 0.1 to 1.9
- out_weight: bfloat16 [2048, 2048], P('tp'), may hold values from -0.125 to 0.125
- gain_post: float32 [2048], P('tp'), may hold values from 0.1 to 1.9
- gate_post: bfloat16 [2048, 5632], P('tp', 'kv'), may hold values from -0.125 to 0.125
- up_post: bfloat16 [2048, 5632], P('tp', 'kv'), may hold values from -0.125 to 0.125
- down_post: bfloat16 [5632, 2048], P('kv', 'tp'), may hold values from -0.078125 to 0.078125
- memory_state: float32 [96, 16, 128, 128], P('kv', 'tp'), may hold values from -4 to 4
Outputs:
- layer_out: bfloat16 [96, 2048], P('kv', 'tp')
- next_state: float32 [96, 16, 128, 128], P('kv', 'tp')
All inputs are finite; a program needn't handle non-finite values.
Results may differ from a plain program's by a relative error of at most 0.014.
Values may be sent and summed in bfloat16 or wider, within the bound.
A program may use at most 64 MiB of HBM per device.

v0:
```python
import functools

import jax
import jax.numpy as jnp
from jax import lax
from jax.experimental import pallas as pl
from jax.experimental.pallas import tpu as pltpu
from jax.sharding import PartitionSpec as P

D = 2048
HEAD_DIM = 128


EPSILON = 1e-06


def channel_mixer(row_block, gain_vec, gate_weight, up_weight, down_weight):
    gathered = lax.all_gather(row_block, "kv", axis=0, tiled=True)
    widened = gathered.astype(jnp.float32)
    part_squares = jnp.sum(widened * widened, axis=1)
    scaled = (widened * gain_vec).astype(jnp.bfloat16)
    gate_part = jnp.dot(scaled, gate_weight, preferred_element_type=jnp.float32)
    up_part = jnp.dot(scaled, up_weight, preferred_element_type=jnp.float32)
    gate_share, up_share, square_share = (
        lax.psum_scatter(
            gate_part.astype(jnp.bfloat16), "tp", scatter_dimension=0, tiled=True
        ).astype(jnp.float32),
        lax.psum_scatter(
            up_part.astype(jnp.bfloat16), "tp", scatter_dimension=0, tiled=True
        ).astype(jnp.float32),
        lax.psum_scatter(
            part_squares.astype(jnp.bfloat16), "tp", scatter_dimension=0, tiled=True
        ).astype(jnp.float32),
    )
    share_inverse = lax.rsqrt(square_share / D + EPSILON)[:, None]
    hidden_share = (jax.nn.silu(gate_share * share_inverse) * (up_share * share_inverse)).astype(
        jnp.bfloat16
    )
    hidden = lax.all_gather(hidden_share, "tp", axis=0, tiled=True)
    return lax.psum_scatter(
        jnp.dot(hidden, down_weight, preferred_element_type=jnp.float32),
        "kv",
        scatter_dimension=0,
        tiled=True,
    )


def token_mixer(
    stream_a,
    gain_mix,
    query_weight,
    forget_weight,
    value_weight,
    outgate_weight,
    lower_bound,
    head_gain,
    out_weight,
    memory_state,
):
    full_rows = lax.all_gather(stream_a, "tp", axis=1, tiled=True)
    widened = full_rows.astype(jnp.float32)
    inverse = lax.rsqrt(jnp.mean(widened * widened, axis=1, keepdims=True) + EPSILON)
    scaled = (widened * gain_mix).astype(jnp.bfloat16)
    weights = (query_weight, forget_weight, value_weight, outgate_weight)
    blocks = lax.all_to_all(scaled, "kv", split_axis=1, concat_axis=0, tiled=True)
    joined = jnp.concatenate(weights, axis=1)
    projected = lax.psum_scatter(
        jnp.dot(blocks, joined, preferred_element_type=jnp.float32),
        "kv",
        scatter_dimension=0,
        tiled=True,
    )
    projected = projected * inverse
    seq_rows = scaled.shape[0]
    local_heads = query_weight.shape[1] // HEAD_DIM
    reshaped = projected.reshape(seq_rows, 4, local_heads, HEAD_DIM)
    query_pre = reshaped[:, 0]
    forget_pre = reshaped[:, 1]
    value_pre = reshaped[:, 2]
    outgate_pre = reshaped[:, 3]
    floor_rate = lower_bound.reshape(local_heads, HEAD_DIM)
    log_keep = jnp.logaddexp(
        jnp.log(floor_rate), jnp.log1p(-floor_rate) + jax.nn.log_sigmoid(forget_pre)
    )
    inject = (1.0 - floor_rate) * jax.nn.sigmoid(-forget_pre)
    next_state = (
        jnp.exp(log_keep)[..., None] * memory_state + inject[..., None] * value_pre[:, :, None, :]
    )
    readout = jnp.einsum(
        "bhk,bhkv->bhv", jax.nn.silu(query_pre), next_state, precision=lax.Precision.HIGHEST
    )
    normed = (
        readout
        * lax.rsqrt(jnp.mean(readout * readout, axis=2, keepdims=True) + EPSILON)
        * head_gain.reshape(local_heads, HEAD_DIM)
    )
    mixed_heads = (
        (normed * jax.nn.silu(outgate_pre))
        .reshape(seq_rows, local_heads * HEAD_DIM)
        .astype(jnp.bfloat16)
    )
    partial_out = jnp.dot(mixed_heads, out_weight, preferred_element_type=jnp.float32)
    mixed = lax.psum_scatter(
        partial_out.astype(jnp.bfloat16), "tp", scatter_dimension=1, tiled=True
    ).astype(jnp.float32)
    return (mixed, next_state)


def shards(
    residual_in,
    gain_pre,
    gate_pre,
    up_pre,
    down_pre,
    gain_mix,
    query_weight,
    forget_weight,
    value_weight,
    outgate_weight,
    lower_bound,
    head_gain,
    out_weight,
    gain_post,
    gate_post,
    up_post,
    down_post,
    memory_state,
):
    branch_a = channel_mixer(residual_in, gain_pre, gate_pre, up_pre, down_pre)
    stream_a = (residual_in.astype(jnp.float32) + 0.5 * branch_a).astype(jnp.bfloat16)
    mixed, next_state = token_mixer(
        stream_a,
        gain_mix,
        query_weight,
        forget_weight,
        value_weight,
        outgate_weight,
        lower_bound,
        head_gain,
        out_weight,
        memory_state,
    )
    stream_b = (stream_a.astype(jnp.float32) + mixed).astype(jnp.bfloat16)
    branch_b = channel_mixer(stream_b, gain_post, gate_post, up_post, down_post)
    layer_out = (stream_b.astype(jnp.float32) + 0.5 * branch_b).astype(jnp.bfloat16)
    return (layer_out, next_state)


ROW_PAD = 8
GATHER_A, SCATTER_A, COLUMNS, PROJECT, GATHER_B, SCATTER_B = 0, 1, 2, 3, 7, 8
KV_EXCHANGES = 9


def dot_columns(rows, weight_columns):
    return lax.dot_general(
        rows, weight_columns, (((1,), (1,)), ((), ())), preferred_element_type=jnp.float32
    )


def fused_layer(
    n_kv,
    residual_ref,
    gain_pre_ref,
    gain_mix_ref,
    lower_ref,
    head_gain_ref,
    gain_post_ref,
    gate_pre_hbm,
    up_pre_hbm,
    down_pre_hbm,
    query_hbm,
    forget_hbm,
    value_hbm,
    outgate_hbm,
    out_hbm,
    gate_post_hbm,
    up_post_hbm,
    down_post_hbm,
    state_hbm,
    layer_ref,
    next_hbm,
    gate_pre,
    up_pre,
    down_pre,
    proj_weights,
    out_weight,
    gate_post,
    up_post,
    down_post,
    state,
    gather_a,
    gather_b,
    partial_a,
    partial_b,
    landed_a,
    landed_b,
    gate_up_out,
    gate_up_in,
    squares_out,
    squares_in,
    stream_out,
    stream_in,
    column_out,
    column_in,
    pair_out,
    pair_in,
    proj_out,
    proj_in,
    mixed_out,
    mixed_in,
    residual_pad,
    sums_pad,
    keep_t,
    inject_t,
    query_t,
    value_rows,
    readout,
    load_sem,
    store_sem,
    kv_send,
    kv_recv,
    tp_send,
    tp_recv,
    pair_send,
    pair_recv,
):
    me = lax.axis_index("kv")
    core = lax.axis_index("tp")
    rows, width = residual_ref.shape
    model = 2 * width
    f32, bf16 = jnp.float32, jnp.bfloat16

    def load(index, source, target):
        return pltpu.make_async_copy(source, target, load_sem.at[index])

    loads = [
        load(0, gate_pre_hbm, gate_pre),
        load(1, up_pre_hbm, up_pre),
        load(2, down_pre_hbm, down_pre),
        load(3, forget_hbm, proj_weights.at[0]),
        load(4, value_hbm, proj_weights.at[1]),
        load(5, query_hbm, proj_weights.at[2]),
        load(6, outgate_hbm, proj_weights.at[3]),
        load(7, state_hbm, state),
        load(8, out_hbm, out_weight),
        load(9, gate_post_hbm, gate_post),
        load(10, up_post_hbm, up_post),
        load(11, down_post_hbm, down_post),
    ]
    for copy in loads:
        copy.start()

    residual_pad[...] = jnp.zeros_like(residual_pad)
    residual_pad[0:rows, :] = residual_ref[...].astype(f32)
    gather_a[me] = residual_pad[...].astype(bf16)
    readout[...] = jnp.zeros_like(readout)
    sums_pad[...] = jnp.zeros_like(sums_pad)

    barrier = pltpu.get_barrier_semaphore()

    def greet(step, carry):
        pl.semaphore_signal(
            barrier,
            inc=1,
            device_id={"kv": lax.rem(me + step, n_kv)},
            device_id_type=pl.DeviceIdType.MESH,
        )
        return carry

    lax.fori_loop(1, n_kv, greet, 0)
    pl.semaphore_signal(
        barrier, inc=1, device_id={"tp": 1 - core}, device_id_type=pl.DeviceIdType.MESH
    )
    pl.semaphore_wait(barrier, n_kv)

    def kv_copy(exchange, source, target, peer, slot):
        return pltpu.make_async_remote_copy(
            src_ref=source,
            dst_ref=target,
            send_sem=kv_send.at[exchange, peer],
            recv_sem=kv_recv.at[exchange, slot],
            device_id={"kv": peer},
            device_id_type=pl.DeviceIdType.MESH,
        )

    def kv_start(exchange, source_of, target):
        def body(step, carry):
            peer = lax.rem(me + step, n_kv)
            kv_copy(exchange, source_of(peer), target.at[me], peer, me).start()
            return carry

        lax.fori_loop(1, n_kv, body, 0)

    def kv_arrive(exchange, target):
        def body(step, carry):
            peer = lax.rem(me + step, n_kv)
            kv_copy(exchange, target.at[peer], target.at[peer], peer, peer).wait_recv()
            return carry

        lax.fori_loop(1, n_kv, body, 0)

    def kv_sent(exchange, source_of, target):
        def body(step, carry):
            peer = lax.rem(me + step, n_kv)
            kv_copy(exchange, source_of(peer), target.at[me], peer, me).wait_send()
            return carry

        lax.fori_loop(1, n_kv, body, 0)

    def tp_copy(index, source, target):
        return pltpu.make_async_remote_copy(
            src_ref=source,
            dst_ref=target,
            send_sem=tp_send.at[index],
            recv_sem=tp_recv.at[index],
            device_id={"tp": 1 - core},
            device_id_type=pl.DeviceIdType.MESH,
        )

    def feed_forward(which, gathered, gain_ref, gate, up, down, partial, landed):
        gather_id, scatter_id = ((GATHER_A, SCATTER_A), (GATHER_B, SCATTER_B))[which]
        kv_start(gather_id, lambda peer: gathered.at[me], gathered)
        for copy in (loads[0:2], loads[9:11])[which]:
            copy.wait()
        kv_arrive(gather_id, gathered)
        wide = gathered[...].astype(f32).reshape(n_kv * ROW_PAD, width)
        squares = jnp.sum(wide * wide, axis=1, keepdims=True)
        squares_out[which] = jnp.broadcast_to(squares, squares_out.shape[1:])
        scaled = (wide * gain_ref[...]).astype(bf16)
        gate_part = dot_columns(scaled, gate[...])
        gate_up_out[which, 0] = gate_part.astype(bf16)
        copies = [
            tp_copy(3 * which, squares_out.at[which], squares_in.at[which]),
            tp_copy(3 * which + 1, gate_up_out.at[which, 0], gate_up_in.at[which, 0]),
            tp_copy(3 * which + 2, gate_up_out.at[which, 1], gate_up_in.at[which, 1]),
        ]
        copies[0].start()
        copies[1].start()
        up_part = dot_columns(scaled, up[...])
        gate_up_out[which, 1] = up_part.astype(bf16)
        copies[2].start()
        for copy in copies:
            copy.wait_recv()
        total = squares + squares_in[which][:, 0:1]
        inverse = lax.rsqrt(total / model + EPSILON)
        gate_sum = (gate_part + gate_up_in[which, 0].astype(f32)) * inverse
        up_sum = (up_part + gate_up_in[which, 1].astype(f32)) * inverse
        hidden = (gate_sum / (1.0 + jnp.exp(-gate_sum)) * up_sum).astype(bf16)
        loads[(2, 11)[which]].wait()
        branch = jnp.dot(hidden, down[...], preferred_element_type=f32)
        partial[...] = branch.reshape(n_kv, ROW_PAD, width)[:, 0:rows, :].astype(bf16)
        landed[me] = partial[me]
        kv_start(scatter_id, lambda peer: partial.at[peer], landed)
        kv_arrive(scatter_id, landed)
        for copy in copies:
            copy.wait_send()
        sums_pad[4 + which, 0:rows, :] = jnp.sum(landed[...].astype(f32), axis=0)
        return sums_pad[4 + which]

    branch_a = feed_forward(
        0, gather_a, gain_pre_ref, gate_pre, up_pre, down_pre, partial_a, landed_a
    )
    stream_a = (residual_pad[...] + 0.5 * branch_a).astype(bf16)

    stream_out[...] = stream_a
    stream_copy = tp_copy(6, stream_out, stream_in)
    stream_copy.start()
    own = stream_a.astype(f32)
    own_squares = jnp.sum(own * own, axis=1, keepdims=True)
    stream_copy.wait_recv()
    other = stream_in[...].astype(f32)
    squares = own_squares + jnp.sum(other * other, axis=1, keepdims=True)
    inverse = lax.rsqrt(squares / model + EPSILON)
    own_scaled = (own * gain_mix_ref[core]).astype(bf16)
    other_scaled = (other * gain_mix_ref[1 - core]).astype(bf16)
    depth = column_out.shape[2]
    half_blocks = n_kv // 2
    for block in range(half_blocks):
        span = slice(block * depth, (block + 1) * depth)
        column_out[core * half_blocks + block] = own_scaled[:, span]
        column_out[(1 - core) * half_blocks + block] = other_scaled[:, span]
    column_in[me] = column_out[me]
    kv_start(COLUMNS, lambda peer: column_out.at[peer], column_in)
    kv_arrive(COLUMNS, column_in)
    columns = column_in[...].astype(f32).reshape(n_kv * ROW_PAD, depth).astype(bf16)
    half = n_kv // 2
    sides = (lax.rem(me, 2), lax.rem(me // 2, 2))
    places = (me // 2, 2 * (me // 4) + lax.rem(me, 2))

    def member(way, place):
        if way == 0:
            return 2 * place + sides[0]
        return 4 * (place // 2) + 2 * sides[1] + lax.rem(place, 2)

    def pair_copy(index):
        way = index % 2
        side = sides[way]
        return pltpu.make_async_remote_copy(
            src_ref=pair_out.at[index, 1 - side],
            dst_ref=pair_in.at[index],
            send_sem=pair_send.at[index],
            recv_sem=pair_recv.at[index],
            device_id={"kv": me + (way + 1) * (1 - 2 * side)},
            device_id_type=pl.DeviceIdType.MESH,
        )

    def side_copy(index, source, target, place, slot):
        return pltpu.make_async_remote_copy(
            src_ref=source,
            dst_ref=target,
            send_sem=kv_send.at[PROJECT + index, place],
            recv_sem=kv_recv.at[PROJECT + index, slot],
            device_id={"kv": member(index % 2, place)},
            device_id_type=pl.DeviceIdType.MESH,
        )

    def side_loop(index, act):
        def body(step, carry):
            act(lax.rem(places[index % 2] + step, half))
            return carry

        lax.fori_loop(1, half, body, 0)

    def side_out(index, place):
        slot = places[index % 2]
        return side_copy(
            index, proj_out.at[index, place], proj_in.at[index, slot], place, slot
        )

    for index in range(4):
        loads[3 + index].wait()
        product = jnp.dot(columns, proj_weights[index], preferred_element_type=f32)
        blocked = product.reshape(n_kv, ROW_PAD, width)[:, 0:rows, :].astype(bf16)
        for block in range(n_kv):
            if index % 2 == 0:
                pair_out[index, block % 2, block // 2] = blocked[block]
            else:
                pair_out[index, block // 2 % 2, 2 * (block // 4) + block % 2] = blocked[block]
        pair_copy(index).start()
    for index in range(4):
        side, slot = sides[index % 2], places[index % 2]
        pair_copy(index).wait_recv()
        proj_out[index] = (
            pair_out[index, side].astype(f32) + pair_in[index].astype(f32)
        ).astype(bf16)
        proj_in[index, slot] = proj_out[index, slot]
        side_loop(index, lambda place, index=index: side_out(index, place).start())

    def projected(index):
        def arrive(place):
            block = proj_in.at[index, place]
            side_copy(index, block, block, place, place).wait_recv()

        side_loop(index, arrive)
        sums_pad[index, 0:rows, :] = jnp.sum(proj_in[index].astype(f32), axis=0)
        return sums_pad[index] * inverse

    heads = width // HEAD_DIM
    floor_rate = lower_ref[...]
    forget_pre = projected(0)
    keep = floor_rate + (1.0 - floor_rate) / (1.0 + jnp.exp(-forget_pre))
    inject = (1.0 - floor_rate) / (1.0 + jnp.exp(forget_pre))
    for head in range(heads):
        span = slice(head * HEAD_DIM, (head + 1) * HEAD_DIM)
        keep_t[head] = keep[:, span].T
        inject_t[head] = inject[:, span].T
    value_pre = projected(1)
    for head in range(heads):
        span = slice(head * HEAD_DIM, (head + 1) * HEAD_DIM)
        value_rows[head] = value_pre[:, span]
    query_pre = projected(2)
    query = query_pre / (1.0 + jnp.exp(-query_pre))
    for head in range(heads):
        span = slice(head * HEAD_DIM, (head + 1) * HEAD_DIM)
        query_t[head] = query[:, span].T
    loads[7].wait()

    def recur(head, carry):
        keep_cols = keep_t[head]
        inject_cols = inject_t[head]
        query_cols = query_t[head]
        values = value_rows[head]
        for row in range(rows):
            col = slice(row, row + 1)
            new = keep_cols[:, col] * state[row, head] + inject_cols[:, col] * values[col, :]
            state[row, head] = new
            readout[head, col, :] = jnp.sum(query_cols[:, col] * new, axis=0, keepdims=True)
        return carry

    lax.fori_loop(0, heads, recur, 0)
    store = pltpu.make_async_copy(state, next_hbm, store_sem)
    outgate_pre = projected(3)
    store.start()
    outgate = outgate_pre / (1.0 + jnp.exp(-outgate_pre))
    mixed_heads = []
    for head in range(heads):
        span = slice(head * HEAD_DIM, (head + 1) * HEAD_DIM)
        read = readout[head]
        scale = lax.rsqrt(jnp.mean(read * read, axis=1, keepdims=True) + EPSILON)
        mixed_heads.append(read * scale * head_gain_ref[:, span] * outgate[:, span])
    mixed_rows = jnp.concatenate(mixed_heads, axis=1).astype(bf16)
    loads[8].wait()
    mixed_part = jnp.dot(mixed_rows, out_weight[...], preferred_element_type=f32)
    mixed_out[0] = mixed_part[:, 0:width]
    mixed_out[1] = mixed_part[:, width:model]
    mixed_copy = tp_copy(7, mixed_out.at[1 - core], mixed_in)
    mixed_copy.start()
    mixed_copy.wait_recv()
    mixed = mixed_out[core] + mixed_in[...]
    stream_b = (stream_out[...].astype(f32) + mixed).astype(bf16)
    gather_b[me] = stream_b
    branch_b = feed_forward(
        1, gather_b, gain_post_ref, gate_post, up_post, down_post, partial_b, landed_b
    )
    layer_out = (gather_b[me].astype(f32) + 0.5 * branch_b).astype(bf16)
    layer_ref[...] = layer_out[0:rows, :]

    stream_copy.wait_send()
    mixed_copy.wait_send()
    kv_sent(GATHER_A, lambda peer: gather_a.at[me], gather_a)
    kv_sent(SCATTER_A, lambda peer: partial_a.at[peer], landed_a)
    kv_sent(COLUMNS, lambda peer: column_out.at[peer], column_in)
    for index in range(4):
        pair_copy(index).wait_send()
        side_loop(index, lambda place, index=index: side_out(index, place).wait_send())
    kv_sent(GATHER_B, lambda peer: gather_b.at[me], gather_b)
    kv_sent(SCATTER_B, lambda peer: partial_b.at[peer], landed_b)
    store.wait()


def fused_shards(
    n_kv,
    residual_in,
    gain_pre,
    gate_pre,
    up_pre,
    down_pre,
    gain_mix,
    query_weight,
    forget_weight,
    value_weight,
    outgate_weight,
    lower_bound,
    head_gain,
    out_weight,
    gain_post,
    gate_post,
    up_post,
    down_post,
    memory_state,
):
    rows, width = residual_in.shape
    depth = query_weight.shape[0]
    hidden = gate_pre.shape[1]
    heads = width // HEAD_DIM
    all_rows = n_kv * ROW_PAD
    f32, bf16 = jnp.float32, jnp.bfloat16
    vmem = pl.BlockSpec(memory_space=pltpu.VMEM)
    hbm = pl.BlockSpec(memory_space=pl.ANY)
    like = lambda array: pltpu.VMEM(array.shape, array.dtype)
    blocks = lambda count: pltpu.VMEM((n_kv, count, width), bf16)
    return pl.pallas_call(
        functools.partial(fused_layer, n_kv),
        out_shape=(
            jax.ShapeDtypeStruct(residual_in.shape, residual_in.dtype),
            jax.ShapeDtypeStruct(memory_state.shape, memory_state.dtype),
        ),
        in_specs=[vmem] * 6 + [hbm] * 12,
        out_specs=(vmem, hbm),
        scratch_shapes=[
            pltpu.VMEM((hidden, width), bf16),
            pltpu.VMEM((hidden, width), bf16),
            like(down_pre),
            pltpu.VMEM((4,) + query_weight.shape, bf16),
            like(out_weight),
            pltpu.VMEM((hidden, width), bf16),
            pltpu.VMEM((hidden, width), bf16),
            like(down_post),
            like(memory_state),
            blocks(ROW_PAD),
            blocks(ROW_PAD),
            blocks(rows),
            blocks(rows),
            blocks(rows),
            blocks(rows),
            pltpu.VMEM((2, 2, all_rows, hidden), bf16),
            pltpu.VMEM((2, 2, all_rows, hidden), bf16),
            pltpu.VMEM((2, all_rows, 128), f32),
            pltpu.VMEM((2, all_rows, 128), f32),
            pltpu.VMEM((ROW_PAD, width), bf16),
            pltpu.VMEM((ROW_PAD, width), bf16),
            pltpu.VMEM((n_kv, ROW_PAD, depth), bf16),
            pltpu.VMEM((n_kv, ROW_PAD, depth), bf16),
            pltpu.VMEM((4, 2, n_kv // 2, rows, width), bf16),
            pltpu.VMEM((4, n_kv // 2, rows, width), bf16),
            pltpu.VMEM((4, n_kv // 2, rows, width), bf16),
            pltpu.VMEM((4, n_kv // 2, rows, width), bf16),
            pltpu.VMEM((2, ROW_PAD, width), f32),
            pltpu.VMEM((ROW_PAD, width), f32),
            pltpu.VMEM((ROW_PAD, width), f32),
            pltpu.VMEM((6, ROW_PAD, width), f32),
            pltpu.VMEM((heads, HEAD_DIM, ROW_PAD), f32),
            pltpu.VMEM((heads, HEAD_DIM, ROW_PAD), f32),
            pltpu.VMEM((heads, HEAD_DIM, ROW_PAD), f32),
            pltpu.VMEM((heads, ROW_PAD, HEAD_DIM), f32),
            pltpu.VMEM((heads, ROW_PAD, HEAD_DIM), f32),
            pltpu.SemaphoreType.DMA((12,)),
            pltpu.SemaphoreType.DMA,
            pltpu.SemaphoreType.DMA((KV_EXCHANGES, n_kv)),
            pltpu.SemaphoreType.DMA((KV_EXCHANGES, n_kv)),
            pltpu.SemaphoreType.DMA((8,)),
            pltpu.SemaphoreType.DMA((8,)),
            pltpu.SemaphoreType.DMA((4,)),
            pltpu.SemaphoreType.DMA((4,)),
        ],
        compiler_params=pltpu.CompilerParams(
            collective_id=0, has_side_effects=True, vmem_limit_bytes=60 * 1024 * 1024
        ),
    )(
        residual_in,
        gain_pre.reshape(1, width),
        gain_mix.reshape(2, 1, width),
        lower_bound.reshape(1, width),
        head_gain.reshape(1, width),
        gain_post.reshape(1, width),
        gate_pre.T,
        up_pre.T,
        down_pre,
        query_weight,
        forget_weight,
        value_weight,
        outgate_weight,
        out_weight,
        gate_post.T,
        up_post.T,
        down_post,
        memory_state,
    )


def solution(mesh):
    n_kv, n_tp = mesh.shape["kv"], mesh.shape["tp"]
    fits = n_tp == 2 and D % (128 * n_kv) == 0 and n_kv % 4 == 0
    body = functools.partial(fused_shards, n_kv) if fits else shards
    in_specs = (
        P("kv", "tp"),
        P("tp"),
        P("tp", "kv"),
        P("tp", "kv"),
        P("kv", "tp"),
        P(),
        P("kv", "tp"),
        P("kv", "tp"),
        P("kv", "tp"),
        P("kv", "tp"),
        P("tp"),
        P("tp"),
        P("tp", None),
        P("tp"),
        P("tp", "kv"),
        P("tp", "kv"),
        P("kv", "tp"),
        P("kv", "tp", None, None),
    )
    out_specs = (P("kv", "tp"), P("kv", "tp", None, None))
    return jax.shard_map(body, mesh=mesh, in_specs=in_specs, out_specs=out_specs, check_vma=False)
```

profile of v0, /device:TPU:0, one launch (start us, length us, event | category | flops | bytes accessed | tf_op | source)
XLA Modules:
  0.0 79.0 jit_solution(17502104514159663366)
XLA Ops:
  0.6 73.1 %shard_map.185 = (bf16[6,1024]{1,0:T(8,128)(2,1)}, f32[6,8,128,128]{3,2,1,0:T(8,128)}) custom-call(bf16[6,1024]{1,0:T(8,128)(2,1)} %residual_ref.1, f32[1,1024]{1,0:T(1,128)} %bitcast.14, f32[2,1,1024]{2,1,0:T(1,128)} %bitcast.13, f32[1,1024]{1,0:T(1,128)} %bitcast.15, f32[1,1024]{1,0:T(1,128)} %bitcast.16, f32[1,1024]{1,0:T(1,128)} %bitcast.17, ...), custom_call_target="tpu_custom_call" | custom-call | tf_op jit(solution)/shard_map/pallas_call | solution.py:562
  73.7 1.3 %copy.22 = bf16[6,1024]{1,0:T(8,128)(2,1)} copy(bf16[6,1024]{1,0:T(8,128)(2,1)} %get-tuple-element.4) | data formatting | bytes 24576
  75.1 3.9 %copy.23 = f32[6,8,128,128]{3,2,1,0:T(8,128)} copy(f32[6,8,128,128]{3,2,1,0:T(8,128)} %get-tuple-element.5) | data formatting | bytes 6291456
where the time goes:
time: 79.3 us; the launch traced here: 79 us
  Pallas kernels  73.1 us (92%)
  local copies, waits for them, and re-layouts  5.23 us (7%)
    pallas_call x1, Pallas kernels, fused_shards(): pl.pallas_call(functools.partial(fused_layer, n_kv), out_shape=(jax.Shape...  73.1 us
    unnamed x2, local copies, waits for them, and re-layouts  5.23 us

commit v1 on v0

v1 whole, which is shorter than its diff:
```python
import functools

import jax
import jax.numpy as jnp
from jax import lax
from jax.experimental import pallas as pl
from jax.experimental.pallas import tpu as pltpu
from jax.sharding import PartitionSpec as P

D = 2048
HEAD_DIM = 128


EPSILON = 1e-06


def channel_mixer(row_block, gain_vec, gate_weight, up_weight, down_weight):
    gathered = lax.all_gather(row_block, "kv", axis=0, tiled=True)
    widened = gathered.astype(jnp.float32)
    part_squares = jnp.sum(widened * widened, axis=1)
    scaled = (widened * gain_vec).astype(jnp.bfloat16)
    gate_part = jnp.dot(scaled, gate_weight, preferred_element_type=jnp.float32)
    up_part = jnp.dot(scaled, up_weight, preferred_element_type=jnp.float32)
    gate_share, up_share, square_share = (
        lax.psum_scatter(
            gate_part.astype(jnp.bfloat16), "tp", scatter_dimension=0, tiled=True
        ).astype(jnp.float32),
        lax.psum_scatter(
            up_part.astype(jnp.bfloat16), "tp", scatter_dimension=0, tiled=True
        ).astype(jnp.float32),
        lax.psum_scatter(
            part_squares.astype(jnp.bfloat16), "tp", scatter_dimension=0, tiled=True
        ).astype(jnp.float32),
    )
    share_inverse = lax.rsqrt(square_share / D + EPSILON)[:, None]
    hidden_share = (jax.nn.silu(gate_share * share_inverse) * (up_share * share_inverse)).astype(
        jnp.bfloat16
    )
    hidden = lax.all_gather(hidden_share, "tp", axis=0, tiled=True)
    return lax.psum_scatter(
        jnp.dot(hidden, down_weight, preferred_element_type=jnp.float32),
        "kv",
        scatter_dimension=0,
        tiled=True,
    )


def token_mixer(
    stream_a,
    gain_mix,
    query_weight,
    forget_weight,
    value_weight,
    outgate_weight,
    lower_bound,
    head_gain,
    out_weight,
    memory_state,
):
    full_rows = lax.all_gather(stream_a, "tp", axis=1, tiled=True)
    widened = full_rows.astype(jnp.float32)
    inverse = lax.rsqrt(jnp.mean(widened * widened, axis=1, keepdims=True) + EPSILON)
    scaled = (widened * gain_mix).astype(jnp.bfloat16)
    weights = (query_weight, forget_weight, value_weight, outgate_weight)
    blocks = lax.all_to_all(scaled, "kv", split_axis=1, concat_axis=0, tiled=True)
    joined = jnp.concatenate(weights, axis=1)
    projected = lax.psum_scatter(
        jnp.dot(blocks, joined, preferred_element_type=jnp.float32),
        "kv",
        scatter_dimension=0,
        tiled=True,
    )
    projected = projected * inverse
    seq_rows = scaled.shape[0]
    local_heads = query_weight.shape[1] // HEAD_DIM
    reshaped = projected.reshape(seq_rows, 4, local_heads, HEAD_DIM)
    query_pre = reshaped[:, 0]
    forget_pre = reshaped[:, 1]
    value_pre = reshaped[:, 2]
    outgate_pre = reshaped[:, 3]
    floor_rate = lower_bound.reshape(local_heads, HEAD_DIM)
    log_keep = jnp.logaddexp(
        jnp.log(floor_rate), jnp.log1p(-floor_rate) + jax.nn.log_sigmoid(forget_pre)
    )
    inject = (1.0 - floor_rate) * jax.nn.sigmoid(-forget_pre)
    next_state = (
        jnp.exp(log_keep)[..., None] * memory_state + inject[..., None] * value_pre[:, :, None, :]
    )
    readout = jnp.einsum(
        "bhk,bhkv->bhv", jax.nn.silu(query_pre), next_state, precision=lax.Precision.HIGHEST
    )
    normed = (
        readout
        * lax.rsqrt(jnp.mean(readout * readout, axis=2, keepdims=True) + EPSILON)
        * head_gain.reshape(local_heads, HEAD_DIM)
    )
    mixed_heads = (
        (normed * jax.nn.silu(outgate_pre))
        .reshape(seq_rows, local_heads * HEAD_DIM)
        .astype(jnp.bfloat16)
    )
    partial_out = jnp.dot(mixed_heads, out_weight, preferred_element_type=jnp.float32)
    mixed = lax.psum_scatter(
        partial_out.astype(jnp.bfloat16), "tp", scatter_dimension=1, tiled=True
    ).astype(jnp.float32)
    return (mixed, next_state)


def shards(
    residual_in,
    gain_pre,
    gate_pre,
    up_pre,
    down_pre,
    gain_mix,
    query_weight,
    forget_weight,
    value_weight,
    outgate_weight,
    lower_bound,
    head_gain,
    out_weight,
    gain_post,
    gate_post,
    up_post,
    down_post,
    memory_state,
):
    branch_a = channel_mixer(residual_in, gain_pre, gate_pre, up_pre, down_pre)
    stream_a = (residual_in.astype(jnp.float32) + 0.5 * branch_a).astype(jnp.bfloat16)
    mixed, next_state = token_mixer(
        stream_a,
        gain_mix,
        query_weight,
        forget_weight,
        value_weight,
        outgate_weight,
        lower_bound,
        head_gain,
        out_weight,
        memory_state,
    )
    stream_b = (stream_a.astype(jnp.float32) + mixed).astype(jnp.bfloat16)
    branch_b = channel_mixer(stream_b, gain_post, gate_post, up_post, down_post)
    layer_out = (stream_b.astype(jnp.float32) + 0.5 * branch_b).astype(jnp.bfloat16)
    return (layer_out, next_state)


LANES = 128
GROUPS = 8
PLANE = 4
GATHER_A, WEIGHTS, SCATTER_A, SHARE, ROWS, PROJECT, GATHER_B, SCATTER_B = range(8)
EXCHANGES = 8
FLIPS = (3, 1, 2, 0)


def dot_columns(rows, weight_columns):
    return lax.dot_general(
        rows, weight_columns, (((1,), (1,)), ((), ())), preferred_element_type=jnp.float32
    )


def lanes(group):
    return slice(group * LANES, (group + 1) * LANES)


def fused_layer(
    n_kv,
    residual_ref,
    gain_pre_ref,
    gain_mix_ref,
    lower_ref,
    head_gain_ref,
    gain_post_ref,
    gate_pre_hbm,
    up_pre_hbm,
    down_pre_hbm,
    query_hbm,
    forget_hbm,
    value_hbm,
    outgate_hbm,
    out_hbm,
    gate_post_hbm,
    up_post_hbm,
    down_post_hbm,
    state_hbm,
    layer_ref,
    next_ref,
    gate_pre,
    up_pre,
    down_pre,
    own_weights,
    plane_weights,
    out_weight,
    gate_post,
    up_post,
    down_post,
    state,
    state_half,
    gather_a,
    gather_b,
    wide_a,
    wide_b,
    spread,
    scaled_rows,
    columns_out,
    columns_landed,
    columns_in,
    rows_out,
    rows_in,
    stream_rows,
    proj_out,
    proj_in,
    inverse_rows,
    keep_t,
    inject_t,
    value_rows,
    mixed_rows,
    mixed_out,
    mixed_in,
    partial_b,
    landed_b,
    gate_up_out,
    gate_up_in,
    squares_out,
    squares_in,
    row_squares_out,
    row_squares_in,
    load_sem,
    send_sem,
    recv_sem,
    tp_send,
    tp_recv,
):
    me = lax.axis_index("kv")
    core = lax.axis_index("tp")
    rows, width = residual_ref.shape
    model = 2 * width
    total = n_kv * rows
    packed = rows * GROUPS
    planes = n_kv // PLANE
    half_planes = planes // 2
    depth_at, spot = me // PLANE, lax.rem(me, PLANE)
    spot_x, spot_y = lax.rem(spot, 2), spot // 2
    slot = lax.rem(me, GROUPS)
    holder = me // GROUPS == core
    f32, bf16 = jnp.float32, jnp.bfloat16

    def flipped(flip):
        return 2 * lax.rem(spot_y + flip // 2, 2) + lax.rem(spot_x + flip % 2, 2)

    def others():
        for step in sorted(range(planes), key=lambda s: -min(s, planes - s)):
            for flip in FLIPS:
                if step or flip:
                    yield lax.rem(depth_at + step, planes) * PLANE + flipped(flip)

    def load(index, source, target):
        return pltpu.make_async_copy(source, target, load_sem.at[index])

    loads = [
        load(0, forget_hbm, own_weights.at[0]),
        load(1, value_hbm, own_weights.at[1]),
        load(2, query_hbm, own_weights.at[2]),
        load(3, outgate_hbm, own_weights.at[3]),
        load(4, gate_pre_hbm, gate_pre),
        load(5, up_pre_hbm, up_pre),
        load(6, down_pre_hbm, down_pre),
        load(7, state_hbm, state),
        load(8, out_hbm, out_weight),
        load(9, gate_post_hbm, gate_post),
        load(10, up_post_hbm, up_post),
        load(11, down_post_hbm, down_post),
    ]
    for copy in loads:
        copy.start()

    def spread_rows(target, values):
        for group in range(GROUPS):
            target[pl.ds(group, values.shape[0], stride=GROUPS), :] = values[:, lanes(group)]

    residual = residual_ref[...].astype(f32)
    spread_rows(stream_rows, residual)
    gather_a[me] = stream_rows[...].astype(bf16)

    barrier = pltpu.get_barrier_semaphore()
    for peer in others():
        pl.semaphore_signal(
            barrier, inc=1, device_id={"kv": peer}, device_id_type=pl.DeviceIdType.MESH
        )
    pl.semaphore_signal(
        barrier, inc=1, device_id={"tp": 1 - core}, device_id_type=pl.DeviceIdType.MESH
    )
    pl.semaphore_wait(barrier, n_kv)

    def remote(exchange, source, target, **device):
        return pltpu.make_async_remote_copy(
            src_ref=source,
            dst_ref=target,
            send_sem=send_sem.at[exchange],
            recv_sem=recv_sem.at[exchange],
            device_id=device,
            device_id_type=pl.DeviceIdType.MESH,
        )

    def all_of(exchange, ref):
        return remote(exchange, ref, ref, tp=1 - core)

    def tp_copy(index, source, target):
        return pltpu.make_async_remote_copy(
            src_ref=source,
            dst_ref=target,
            send_sem=tp_send.at[index],
            recv_sem=tp_recv.at[index],
            device_id={"tp": 1 - core},
            device_id_type=pl.DeviceIdType.MESH,
        )

    def feed_forward(which, gathered, wide, gain_ref, gate, up, down):
        wide[...] = gathered[...].astype(f32).reshape(n_kv * packed, LANES)
        square_lanes = jnp.zeros((total, LANES), f32)
        for group in range(GROUPS):
            part = wide[pl.ds(group, total, stride=GROUPS), :]
            square_lanes += part * part
            scaled_rows[:, lanes(group)] = (part * gain_ref[:, lanes(group)]).astype(bf16)
        scaled = scaled_rows[...]
        squares = jnp.sum(square_lanes, axis=1, keepdims=True)
        squares_out[which] = jnp.broadcast_to(squares, squares_out.shape[1:])
        gate_part = dot_columns(scaled, gate[...])
        gate_up_out[which, 0] = gate_part.astype(bf16)
        copies = [
            tp_copy(3 * which, squares_out.at[which], squares_in.at[which]),
            tp_copy(3 * which + 1, gate_up_out.at[which, 0], gate_up_in.at[which, 0]),
            tp_copy(3 * which + 2, gate_up_out.at[which, 1], gate_up_in.at[which, 1]),
        ]
        copies[0].start()
        copies[1].start()
        up_part = dot_columns(scaled, up[...])
        gate_up_out[which, 1] = up_part.astype(bf16)
        copies[2].start()
        for copy in copies:
            copy.wait_recv()
        inverse = lax.rsqrt((squares + squares_in[which][:, 0:1]) / model + EPSILON)
        gate_sum = (gate_part + gate_up_in[which, 0].astype(f32)) * inverse
        up_sum = (up_part + gate_up_in[which, 1].astype(f32)) * inverse
        hidden = (gate_sum / (1.0 + jnp.exp(-gate_sum)) * up_sum).astype(bf16)
        return jnp.dot(hidden, down[...], preferred_element_type=f32), copies

    def gather_start(exchange, gathered):
        for peer in others():
            remote(exchange, gathered.at[me], gathered.at[me], kv=peer).start()

    def but_one(ref):
        return ref.at[pl.ds(0, n_kv - 1)]

    gather_start(GATHER_A, gather_a)
    for copy in loads[0:4]:
        copy.wait()
    for flip in FLIPS[:-1]:
        peer_spot = flipped(flip)
        remote(
            WEIGHTS,
            own_weights.at[peer_spot],
            plane_weights.at[spot],
            kv=depth_at * PLANE + peer_spot,
        ).start()
    plane_weights[spot] = own_weights[spot]
    mixed_rows[packed:, :] = jnp.zeros((mixed_rows.shape[0] - packed, LANES), f32)
    for copy in loads[4:7]:
        copy.wait()
    all_of(GATHER_A, but_one(gather_a)).wait_recv()
    branch_a, copies_a = feed_forward(
        0, gather_a, wide_a, gain_pre_ref, gate_pre, up_pre, down_pre
    )
    for group in range(GROUPS):
        columns_out[group] = branch_a[:, lanes(group)].astype(bf16)
    for flip in FLIPS:
        for step in range(half_planes - 1, -1, -1):
            plane = core * half_planes + lax.rem(depth_at + step, half_planes)
            peer = plane * PLANE + flipped(flip)
            copy = remote(
                SCATTER_A, columns_out.at[lax.rem(peer, GROUPS)], columns_landed.at[me], kv=peer
            )
            if step or flip:
                copy.start()
            else:
                pl.when(jnp.logical_not(holder))(copy.start)

    @pl.when(holder)
    def _():
        columns_landed[me] = columns_out[slot]
        all_of(SCATTER_A, but_one(columns_landed)).wait_recv()
        branch = jnp.sum(columns_landed[...].astype(f32), axis=0)
        shared = wide_a[pl.ds(slot, total, stride=GROUPS), :]
        stream = (shared + 0.5 * branch).astype(bf16).astype(f32)
        columns_in[spot] = (stream * gain_mix_ref[me]).astype(bf16)
        block = columns_in.at[spot]
        for flip in FLIPS:
            peer = depth_at * PLANE + flipped(flip)
            if flip:
                remote(SHARE, block, block, kv=peer, tp=core).start()
            remote(SHARE, block, block, kv=peer, tp=1 - core).start()
        for owner in range(n_kv):
            rows_out[owner] = stream[owner * rows : (owner + 1) * rows, :]
        for peer in others():
            remote(ROWS, rows_out.at[peer], rows_in.at[slot], kv=peer).start()
        rows_in[slot] = rows_out[me]
        all_of(SHARE, columns_in.at[pl.ds(0, PLANE - 1)]).wait_recv()

    @pl.when(jnp.logical_not(holder))
    def _():
        all_of(SHARE, columns_in).wait_recv()

    all_of(WEIGHTS, plane_weights.at[pl.ds(0, PLANE - 1)]).wait_recv()
    columns = jnp.concatenate([columns_in[part] for part in range(PLANE)], axis=1)
    product = jnp.dot(
        columns,
        plane_weights[...].reshape(PLANE * LANES, width),
        preferred_element_type=f32,
    )
    spread_rows(spread, product)
    proj_out[...] = spread[...].astype(bf16).reshape(n_kv, packed, LANES)
    for peer in others():
        remote(PROJECT, proj_out.at[peer], proj_in.at[me], kv=peer).start()
    proj_in[me] = proj_out[me]

    @pl.when(holder)
    def _():
        all_of(ROWS, rows_in.at[pl.ds(0, GROUPS - 1)]).wait_recv()

    @pl.when(jnp.logical_not(holder))
    def _():
        all_of(ROWS, rows_in).wait_recv()

    for group in range(GROUPS):
        stream_rows[pl.ds(group, rows, stride=GROUPS), :] = rows_in[group]
    stream = stream_rows[...].reshape(rows, GROUPS, LANES)
    row_squares = jnp.sum(stream * stream, axis=1)
    row_squares_out[...] = row_squares
    square_copy = tp_copy(6, row_squares_out, row_squares_in)
    square_copy.start()
    loads[7].wait()
    for row in range(rows):
        for head in range(GROUPS):
            state_half[row // 2, head * LANES : (head + 1) * LANES, lanes(row % 2)] = state[
                row, head
            ].astype(bf16)
    square_copy.wait_recv()
    squares = jnp.sum(row_squares + row_squares_in[...], axis=1, keepdims=True)
    inverse = lax.rsqrt(squares / model + EPSILON)
    for row in range(rows):
        inverse_rows[row * GROUPS : (row + 1) * GROUPS, :] = jnp.broadcast_to(
            inverse[row : row + 1, :], (GROUPS, LANES)
        )
    loads[8].wait()
    all_of(PROJECT, but_one(proj_in)).wait_recv()

    def projected(index):
        parts = [proj_in[plane * PLANE + index].astype(f32) for plane in range(planes)]
        return sum(parts[1:], parts[0]) * inverse_rows[...]

    floor_rate = jnp.concatenate([lower_ref[...]] * rows, axis=0)
    forget_pre = projected(0)
    keep = floor_rate + (1.0 - floor_rate) / (1.0 + jnp.exp(-forget_pre))
    inject = (1.0 - floor_rate) / (1.0 + jnp.exp(forget_pre))
    query_pre = projected(2)
    query = query_pre / (1.0 + jnp.exp(-query_pre))
    value = projected(1)
    value_rows[...] = value
    weighted = query * keep
    direct = jnp.sum(query * inject, axis=1, keepdims=True) * value
    head_index = lax.broadcasted_iota(jnp.int32, (GROUPS, LANES), 0)
    read = []
    for pair in range(rows // 2):
        diagonal = []
        for row in (2 * pair, 2 * pair + 1):
            heads = weighted[row * GROUPS : (row + 1) * GROUPS, :]
            diagonal.append(
                jnp.concatenate(
                    [jnp.where(head_index == head, heads, 0.0) for head in range(GROUPS)], axis=1
                )
            )
        both = jnp.dot(
            jnp.concatenate(diagonal, axis=0).astype(bf16),
            state_half[pair],
            preferred_element_type=f32,
        )
        read.append(both[0:GROUPS, lanes(0)])
        read.append(both[GROUPS : 2 * GROUPS, lanes(1)])
    readout = jnp.concatenate(read, axis=0) + direct
    outgate_pre = projected(3)
    outgate = outgate_pre / (1.0 + jnp.exp(-outgate_pre))
    scale = lax.rsqrt(jnp.mean(readout * readout, axis=1, keepdims=True) + EPSILON)
    head_gain = jnp.concatenate([head_gain_ref[...]] * rows, axis=0)
    mixed_rows[0:packed, :] = readout * scale * head_gain * outgate
    mixed_heads = jnp.concatenate(
        [mixed_rows[pl.ds(head, GROUPS, stride=GROUPS), :] for head in range(GROUPS)], axis=1
    ).astype(bf16)
    mixed_part = jnp.dot(mixed_heads, out_weight[...], preferred_element_type=f32)[0:rows]
    for half in range(2):
        spread_rows(mixed_out.at[half], mixed_part[:, half * width : (half + 1) * width])
    mixed_copy = tp_copy(7, mixed_out.at[1 - core], mixed_in)
    mixed_copy.start()
    for row in range(rows):
        span = slice(row * GROUPS, (row + 1) * GROUPS)
        keep_t[row] = keep[span].T
        inject_t[row] = inject[span].T
    mixed_copy.wait_recv()
    stream_b = (stream_rows[...] + (mixed_out[core] + mixed_in[...])).astype(bf16)
    gather_b[me] = stream_b
    gather_start(GATHER_B, gather_b)

    def update(row, carry):
        keep_columns = keep_t[row]
        inject_columns = inject_t[row]
        for head in range(GROUPS):
            column = slice(head, head + 1)
            values = value_rows[pl.ds(row * GROUPS + head, 1), :]
            next_ref[row, head] = (
                keep_columns[:, column] * state[row, head] + inject_columns[:, column] * values
            )
        return carry

    lax.fori_loop(0, rows, update, 0)
    for copy in loads[9:12]:
        copy.wait()
    all_of(GATHER_B, but_one(gather_b)).wait_recv()
    branch_b, copies_b = feed_forward(
        1, gather_b, wide_b, gain_post_ref, gate_post, up_post, down_post
    )
    spread_rows(spread, branch_b)
    partial_b[...] = spread[...].astype(bf16).reshape(n_kv, packed, LANES)
    for peer in others():
        remote(SCATTER_B, partial_b.at[peer], landed_b.at[me], kv=peer).start()
    landed_b[me] = partial_b[me]
    for copy in copies_a + copies_b + [square_copy, mixed_copy]:
        copy.wait_send()
    all_of(GATHER_A, but_one(gather_a)).wait_send()
    all_of(WEIGHTS, plane_weights.at[pl.ds(0, PLANE - 1)]).wait_send()
    all_of(PROJECT, but_one(proj_out)).wait_send()
    all_of(GATHER_B, but_one(gather_b)).wait_send()

    @pl.when(holder)
    def _():
        all_of(SCATTER_A, columns_out.at[pl.ds(0, GROUPS - 1)]).wait_send()
        all_of(SHARE, columns_landed.at[pl.ds(0, 2 * PLANE - 1)]).wait_send()
        all_of(ROWS, but_one(rows_out)).wait_send()

    @pl.when(jnp.logical_not(holder))
    def _():
        all_of(SCATTER_A, columns_out).wait_send()

    all_of(SCATTER_B, but_one(landed_b)).wait_recv()
    branch = jnp.sum(landed_b[...].astype(f32), axis=0)
    spread[0:packed, :] = gather_b[me].astype(f32) + 0.5 * branch
    for group in range(GROUPS):
        layer_ref[:, lanes(group)] = spread[pl.ds(group, rows, stride=GROUPS), :].astype(bf16)
    all_of(SCATTER_B, but_one(partial_b)).wait_send()


def store_results(layer_in, state_in, layer_out, state_out, sem):
    copies = [pltpu.make_async_copy(layer_in, layer_out, sem.at[0])]
    for row in range(state_in.shape[0]):
        copies.append(pltpu.make_async_copy(state_in.at[row], state_out.at[row], sem.at[1 + row]))
    for copy in copies:
        copy.start()
    for copy in copies:
        copy.wait()


def fused_shards(
    n_kv,
    residual_in,
    gain_pre,
    gate_pre,
    up_pre,
    down_pre,
    gain_mix,
    query_weight,
    forget_weight,
    value_weight,
    outgate_weight,
    lower_bound,
    head_gain,
    out_weight,
    gain_post,
    gate_post,
    up_post,
    down_post,
    memory_state,
):
    rows, width = residual_in.shape
    hidden = gate_pre.shape[1]
    total = n_kv * rows
    packed = rows * GROUPS
    f32, bf16 = jnp.float32, jnp.bfloat16
    vmem = pl.BlockSpec(memory_space=pltpu.VMEM)
    hbm = pl.BlockSpec(memory_space=pltpu.HBM)
    like = lambda array: pltpu.VMEM(array.shape, array.dtype)
    blocks = lambda: pltpu.VMEM((n_kv, packed, LANES), bf16)
    outs = (
        jax.ShapeDtypeStruct(residual_in.shape, residual_in.dtype),
        jax.ShapeDtypeStruct(memory_state.shape, memory_state.dtype),
    )
    layer, state = pl.pallas_call(
        functools.partial(fused_layer, n_kv),
        out_shape=tuple(pltpu.VMEM(out.shape, out.dtype) for out in outs),
        in_specs=[vmem] * 6 + [hbm] * 12,
        out_specs=(vmem, vmem),
        scratch_shapes=[
            pltpu.VMEM((hidden, width), bf16),
            pltpu.VMEM((hidden, width), bf16),
            like(down_pre),
            pltpu.VMEM((PLANE,) + query_weight.shape, bf16),
            pltpu.VMEM((PLANE,) + query_weight.shape, bf16),
            like(out_weight),
            pltpu.VMEM((hidden, width), bf16),
            pltpu.VMEM((hidden, width), bf16),
            like(down_post),
            like(memory_state),
            pltpu.VMEM((rows // 2, width, 2 * LANES), bf16),
            blocks(),
            blocks(),
            pltpu.VMEM((n_kv * packed, LANES), f32),
            pltpu.VMEM((n_kv * packed, LANES), f32),
            pltpu.VMEM((n_kv * packed, LANES), f32),
            pltpu.VMEM((total, width), bf16),
            pltpu.VMEM((GROUPS, total, LANES), bf16),
            pltpu.VMEM((n_kv, total, LANES), bf16),
            pltpu.VMEM((PLANE, total, LANES), bf16),
            pltpu.VMEM((n_kv, rows, LANES), f32),
            pltpu.VMEM((GROUPS, rows, LANES), f32),
            pltpu.VMEM((packed, LANES), f32),
            blocks(),
            blocks(),
            pltpu.VMEM((packed, LANES), f32),
            pltpu.VMEM((rows, LANES, GROUPS), f32),
            pltpu.VMEM((rows, LANES, GROUPS), f32),
            pltpu.VMEM((packed, LANES), f32),
            pltpu.VMEM((GROUPS * GROUPS, LANES), f32),
            pltpu.VMEM((2, packed, LANES), f32),
            pltpu.VMEM((packed, LANES), f32),
            blocks(),
            blocks(),
            pltpu.VMEM((2, 2, total, hidden), bf16),
            pltpu.VMEM((2, 2, total, hidden), bf16),
            pltpu.VMEM((2, total, LANES), f32),
            pltpu.VMEM((2, total, LANES), f32),
            pltpu.VMEM((rows, LANES), f32),
            pltpu.VMEM((rows, LANES), f32),
            pltpu.SemaphoreType.DMA((12,)),
            pltpu.SemaphoreType.DMA((EXCHANGES,)),
            pltpu.SemaphoreType.DMA((EXCHANGES,)),
            pltpu.SemaphoreType.DMA((8,)),
            pltpu.SemaphoreType.DMA((8,)),
        ],
        compiler_params=pltpu.CompilerParams(
            collective_id=0, has_side_effects=True, vmem_limit_bytes=56 * 1024 * 1024
        ),
    )(
        residual_in,
        gain_pre.reshape(1, width),
        gain_mix.reshape(n_kv, 1, LANES),
        lower_bound.reshape(GROUPS, LANES),
        head_gain.reshape(GROUPS, LANES),
        gain_post.reshape(1, width),
        gate_pre.T,
        up_pre.T,
        down_pre,
        query_weight,
        forget_weight,
        value_weight,
        outgate_weight,
        out_weight,
        gate_post.T,
        up_post.T,
        down_post,
        memory_state,
    )
    return pl.pallas_call(
        store_results,
        out_shape=outs,
        in_specs=[vmem, vmem],
        out_specs=(hbm, hbm),
        scratch_shapes=[pltpu.SemaphoreType.DMA((1 + rows,))],
        compiler_params=pltpu.CompilerParams(vmem_limit_bytes=8 * 1024 * 1024),
    )(layer, state)


def solution(mesh):
    n_kv, n_tp = mesh.shape["kv"], mesh.shape["tp"]
    fits = n_tp == 2 and n_kv * LANES == D and n_kv // n_tp == GROUPS
    body = functools.partial(fused_shards, n_kv) if fits else shards
    in_specs = (
        P("kv", "tp"),
        P("tp"),
        P("tp", "kv"),
        P("tp", "kv"),
        P("kv", "tp"),
        P(),
        P("kv", "tp"),
        P("kv", "tp"),
        P("kv", "tp"),
        P("kv", "tp"),
        P("tp"),
        P("tp"),
        P("tp", None),
        P("tp"),
        P("tp", "kv"),
        P("tp", "kv"),
        P("kv", "tp"),
        P("kv", "tp", None, None),
    )
    out_specs = (P("kv", "tp"), P("kv", "tp", None, None))
    return jax.shard_map(body, mesh=mesh, in_specs=in_specs, out_specs=out_specs, check_vma=False)
```

time: 79.3 us -> 52.9 us (0.67)
  Pallas kernels: 73.1 us -> 52.1 us
  local copies, waits for them, and re-layouts: 5.23 us -> 0 us
    pallas_call x1 -> x2, Pallas kernels: 73.1 us -> 52.1 us  [the longest x1 50.3 us: fused_shards(): pl.pallas_call(functools.partial(fused_layer, n_kv), out_shape=tuple((plt...]
    unnamed x2 -> x0, local copies, waits for them, and re-layouts: 5.23 us -> none
where the time goes in v1:
time: 52.9 us; the launch traced here: 52.7 us
  Pallas kernels  52.1 us (98%)
  between operations  0.65 us (1%)
    pallas_call x1, Pallas kernels, fused_shards(): pl.pallas_call(functools.partial(fused_layer, n_kv), out_shape=tuple((plt...  50.3 us
    pallas_call x1, Pallas kernels, fused_shards(): pl.pallas_call(store_results, out_shape=outs, in_specs=[vmem, vmem], out_...  1.72 us

profile of v1, /device:TPU:0, one launch (start us, length us, event | category | flops | bytes accessed | tf_op | source)
XLA Modules:
  0.0 52.7 jit_solution(9600115278006347669)
XLA Ops:
  0.6 50.3 %shard_map.185 = (bf16[6,1024]{1,0:T(8,128)(2,1)S(1)}, f32[6,8,128,128]{3,2,1,0:T(8,128)S(1)}) custom-call(bf16[6,1024]{1,0:T(8,128)(2,1)} %residual_ref.1, f32[1,1024]{1,0:T(1,128)} %bitcast.14, f32[16,1,128]{2,1,0:T(1,128)} %bitcast.13, f32[8,128]{1,0:T(8,128)} %bitcast.15, f32[8,128]{1,0:T(8,128)} %bitcast.16, f32[1,1024]{1,0:T(1,128)} %bitcast.17, ...), custom_call_target="tpu_custom_call" | custom-call | tf_op jit(solution)/shard_map/pallas_call | solution.py:605
  51.0 1.7 %shard_map.186 = (bf16[6,1024]{1,0:T(8,128)(2,1)}, f32[6,8,128,128]{3,2,1,0:T(8,128)}) custom-call(bf16[6,1024]{1,0:T(8,128)(2,1)S(1)} %get-tuple-element.4.layer_in, f32[6,8,128,128]{3,2,1,0:T(8,128)S(1)} %get-tuple-element.5.state_in), custom_call_target="tpu_custom_call" | custom-call | tf_op jit(solution)/shard_map/pallas_call | solution.py:680

commit v2 on v1

--- a/solution.py
+++ b/solution.py
@@ -151,13 +151,8 @@
 PLANE = 4
 GATHER_A, WEIGHTS, SCATTER_A, SHARE, ROWS, PROJECT, GATHER_B, SCATTER_B = range(8)
 EXCHANGES = 8
+HOLDER = 1
 FLIPS = (3, 1, 2, 0)
-
-
-def dot_columns(rows, weight_columns):
-    return lax.dot_general(
-        rows, weight_columns, (((1,), (1,)), ((), ())), preferred_element_type=jnp.float32
-    )
 
 
 def lanes(group):
@@ -195,6 +190,10 @@
     gate_post,
     up_post,
     down_post,
+    gate_pre_t,
+    up_pre_t,
+    gate_post_t,
+    up_post_t,
     state,
     state_half,
     gather_a,
@@ -206,6 +205,8 @@
     columns_out,
     columns_landed,
     columns_in,
+    shared_out,
+    shared_in,
     rows_out,
     rows_in,
     stream_rows,
@@ -217,6 +218,7 @@
     value_rows,
     mixed_rows,
     mixed_out,
+    mixed_own,
     mixed_in,
     partial_b,
     landed_b,
@@ -243,17 +245,20 @@
     depth_at, spot = me // PLANE, lax.rem(me, PLANE)
     spot_x, spot_y = lax.rem(spot, 2), spot // 2
     slot = lax.rem(me, GROUPS)
-    holder = me // GROUPS == core
+    owner_core = me // GROUPS
+    holder = core == HOLDER
+    owns = jnp.logical_and(holder, owner_core == HOLDER)
     f32, bf16 = jnp.float32, jnp.bfloat16
 
     def flipped(flip):
         return 2 * lax.rem(spot_y + flip // 2, 2) + lax.rem(spot_x + flip % 2, 2)
 
     def others():
-        for step in sorted(range(planes), key=lambda s: -min(s, planes - s)):
-            for flip in FLIPS:
+        for flip in FLIPS:
+            for step in range(planes - 1, -1, -1):
+                plane = 2 * lax.rem(depth_at // 2 + step // 2, 2) + lax.rem(depth_at + step, 2)
                 if step or flip:
-                    yield lax.rem(depth_at + step, planes) * PLANE + flipped(flip)
+                    yield plane * PLANE + flipped(flip)
 
     def load(index, source, target):
         return pltpu.make_async_copy(source, target, load_sem.at[index])
@@ -267,7 +272,8 @@
         load(5, up_pre_hbm, up_pre),
         load(6, down_pre_hbm, down_pre),
         load(7, state_hbm, state),
-        load(8, out_hbm, out_weight),
+        load(8, out_hbm.at[:, pl.ds(0, width)], out_weight.at[0]),
+        load(12, out_hbm.at[:, pl.ds(width, width)], out_weight.at[1]),
         load(9, gate_post_hbm, gate_post),
         load(10, up_post_hbm, up_post),
         load(11, down_post_hbm, down_post),
@@ -326,7 +332,7 @@
         scaled = scaled_rows[...]
         squares = jnp.sum(square_lanes, axis=1, keepdims=True)
         squares_out[which] = jnp.broadcast_to(squares, squares_out.shape[1:])
-        gate_part = dot_columns(scaled, gate[...])
+        gate_part = jnp.dot(scaled, gate[...], preferred_element_type=f32)
         gate_up_out[which, 0] = gate_part.astype(bf16)
         copies = [
             tp_copy(3 * which, squares_out.at[which], squares_in.at[which]),
@@ -335,7 +341,7 @@
         ]
         copies[0].start()
         copies[1].start()
-        up_part = dot_columns(scaled, up[...])
+        up_part = jnp.dot(scaled, up[...], preferred_element_type=f32)
         gate_up_out[which, 1] = up_part.astype(bf16)
         copies[2].start()
         for copy in copies:
@@ -349,6 +355,10 @@
     def gather_start(exchange, gathered):
         for peer in others():
             remote(exchange, gathered.at[me], gathered.at[me], kv=peer).start()
+
+    def turn(target, source):
+        for group in range(GROUPS):
+            target[lanes(group), :] = source[:, lanes(group)].T
 
     def but_one(ref):
         return ref.at[pl.ds(0, n_kv - 1)]
@@ -368,43 +378,75 @@
     mixed_rows[packed:, :] = jnp.zeros((mixed_rows.shape[0] - packed, LANES), f32)
     for copy in loads[4:7]:
         copy.wait()
+    turn(gate_pre_t, gate_pre)
+    turn(up_pre_t, up_pre)
     all_of(GATHER_A, but_one(gather_a)).wait_recv()
     branch_a, copies_a = feed_forward(
-        0, gather_a, wide_a, gain_pre_ref, gate_pre, up_pre, down_pre
+        0, gather_a, wide_a, gain_pre_ref, gate_pre_t, up_pre_t, down_pre
     )
     for group in range(GROUPS):
         columns_out[group] = branch_a[:, lanes(group)].astype(bf16)
+    shared_copy = tp_copy(8, shared_out, shared_in)
+
+    @pl.when(owner_core == core)
+    def _():
+        shared_out[...] = wide_a[pl.ds(slot, total, stride=GROUPS), :].astype(bf16)
+
+        @pl.when(jnp.logical_not(holder))
+        def _():
+            shared_copy.start()
+
     for flip in FLIPS:
         for step in range(half_planes - 1, -1, -1):
             plane = core * half_planes + lax.rem(depth_at + step, half_planes)
             peer = plane * PLANE + flipped(flip)
             copy = remote(
-                SCATTER_A, columns_out.at[lax.rem(peer, GROUPS)], columns_landed.at[me], kv=peer
+                SCATTER_A,
+                columns_out.at[lax.rem(peer, GROUPS)],
+                columns_landed.at[me],
+                kv=peer,
+                tp=HOLDER,
             )
             if step or flip:
                 copy.start()
             else:
-                pl.when(jnp.logical_not(holder))(copy.start)
+                pl.when(jnp.logical_not(owns))(copy.start)
 
     @pl.when(holder)
     def _():
-        columns_landed[me] = columns_out[slot]
-        all_of(SCATTER_A, but_one(columns_landed)).wait_recv()
+        @pl.when(owns)
+        def _():
+            columns_landed[me] = columns_out[slot]
+            all_of(SCATTER_A, but_one(columns_landed)).wait_recv()
+            shared_in[...] = shared_out[...]
+
+        @pl.when(jnp.logical_not(owns))
+        def _():
+            all_of(SCATTER_A, columns_landed).wait_recv()
+            shared_copy.wait_recv()
+
         branch = jnp.sum(columns_landed[...].astype(f32), axis=0)
-        shared = wide_a[pl.ds(slot, total, stride=GROUPS), :]
-        stream = (shared + 0.5 * branch).astype(bf16).astype(f32)
+        stream = (shared_in[...].astype(f32) + 0.5 * branch).astype(bf16).astype(f32)
         columns_in[spot] = (stream * gain_mix_ref[me]).astype(bf16)
         block = columns_in.at[spot]
         for flip in FLIPS:
             peer = depth_at * PLANE + flipped(flip)
+            remote(SHARE, block, block, kv=peer, tp=1 - core).start()
             if flip:
                 remote(SHARE, block, block, kv=peer, tp=core).start()
-            remote(SHARE, block, block, kv=peer, tp=1 - core).start()
         for owner in range(n_kv):
             rows_out[owner] = stream[owner * rows : (owner + 1) * rows, :]
         for peer in others():
-            remote(ROWS, rows_out.at[peer], rows_in.at[slot], kv=peer).start()
-        rows_in[slot] = rows_out[me]
+            remote(ROWS, rows_out.at[peer], rows_in.at[slot], kv=peer, tp=owner_core).start()
+
+        @pl.when(owns)
+        def _():
+            rows_in[slot] = rows_out[me]
+
+        @pl.when(jnp.logical_not(owns))
+        def _():
+            remote(ROWS, rows_out.at[me], rows_in.at[slot], tp=1 - core).start()
+
         all_of(SHARE, columns_in.at[pl.ds(0, PLANE - 1)]).wait_recv()
 
     @pl.when(jnp.logical_not(holder))
@@ -424,11 +466,11 @@
         remote(PROJECT, proj_out.at[peer], proj_in.at[me], kv=peer).start()
     proj_in[me] = proj_out[me]
 
-    @pl.when(holder)
+    @pl.when(owns)
     def _():
         all_of(ROWS, rows_in.at[pl.ds(0, GROUPS - 1)]).wait_recv()
 
-    @pl.when(jnp.logical_not(holder))
+    @pl.when(jnp.logical_not(owns))
     def _():
         all_of(ROWS, rows_in).wait_recv()
 
@@ -445,6 +487,10 @@
             state_half[row // 2, head * LANES : (head + 1) * LANES, lanes(row % 2)] = state[
                 row, head
             ].astype(bf16)
+    for copy in loads[10:12]:
+        copy.wait()
+    turn(gate_post_t, gate_post)
+    turn(up_post_t, up_post)
     square_copy.wait_recv()
     squares = jnp.sum(row_squares + row_squares_in[...], axis=1, keepdims=True)
     inverse = lax.rsqrt(squares / model + EPSILON)
@@ -453,6 +499,7 @@
             inverse[row : row + 1, :], (GROUPS, LANES)
         )
     loads[8].wait()
+    loads[9].wait()
     all_of(PROJECT, but_one(proj_in)).wait_recv()
 
     def projected(index):
@@ -496,17 +543,18 @@
     mixed_heads = jnp.concatenate(
         [mixed_rows[pl.ds(head, GROUPS, stride=GROUPS), :] for head in range(GROUPS)], axis=1
     ).astype(bf16)
-    mixed_part = jnp.dot(mixed_heads, out_weight[...], preferred_element_type=f32)[0:rows]
-    for half in range(2):
-        spread_rows(mixed_out.at[half], mixed_part[:, half * width : (half + 1) * width])
-    mixed_copy = tp_copy(7, mixed_out.at[1 - core], mixed_in)
+    away = jnp.dot(mixed_heads, out_weight[1 - core], preferred_element_type=f32)
+    spread_rows(mixed_out, away[0:rows])
+    mixed_copy = tp_copy(7, mixed_out, mixed_in)
     mixed_copy.start()
+    home = jnp.dot(mixed_heads, out_weight[core], preferred_element_type=f32)
+    spread_rows(mixed_own, home[0:rows])
     for row in range(rows):
         span = slice(row * GROUPS, (row + 1) * GROUPS)
         keep_t[row] = keep[span].T
         inject_t[row] = inject[span].T
     mixed_copy.wait_recv()
-    stream_b = (stream_rows[...] + (mixed_out[core] + mixed_in[...])).astype(bf16)
+    stream_b = (stream_rows[...] + (mixed_own[...] + mixed_in[...])).astype(bf16)
     gather_b[me] = stream_b
     gather_start(GATHER_B, gather_b)
 
@@ -522,11 +570,10 @@
         return carry
 
     lax.fori_loop(0, rows, update, 0)
-    for copy in loads[9:12]:
-        copy.wait()
+    loads[12].wait()
     all_of(GATHER_B, but_one(gather_b)).wait_recv()
     branch_b, copies_b = feed_forward(
-        1, gather_b, wide_b, gain_post_ref, gate_post, up_post, down_post
+        1, gather_b, wide_b, gain_post_ref, gate_post_t, up_post_t, down_post
     )
     spread_rows(spread, branch_b)
     partial_b[...] = spread[...].astype(bf16).reshape(n_kv, packed, LANES)
@@ -542,13 +589,24 @@
 
     @pl.when(holder)
     def _():
+        all_of(SHARE, columns_landed.at[pl.ds(0, 2 * PLANE - 1)]).wait_send()
+
+    @pl.when(owns)
+    def _():
         all_of(SCATTER_A, columns_out.at[pl.ds(0, GROUPS - 1)]).wait_send()
-        all_of(SHARE, columns_landed.at[pl.ds(0, 2 * PLANE - 1)]).wait_send()
         all_of(ROWS, but_one(rows_out)).wait_send()
 
-    @pl.when(jnp.logical_not(holder))
+    @pl.when(jnp.logical_not(owns))
     def _():
         all_of(SCATTER_A, columns_out).wait_send()
+
+        @pl.when(holder)
+        def _():
+            all_of(ROWS, rows_out).wait_send()
+
+    @pl.when(jnp.logical_and(owner_core == core, jnp.logical_not(holder)))
+    def _():
+        shared_copy.wait_send()
 
     all_of(SCATTER_B, but_one(landed_b)).wait_recv()
     branch = jnp.sum(landed_b[...].astype(f32), axis=0)
@@ -613,10 +671,14 @@
             like(down_pre),
             pltpu.VMEM((PLANE,) + query_weight.shape, bf16),
             pltpu.VMEM((PLANE,) + query_weight.shape, bf16),
-            like(out_weight),
+            pltpu.VMEM((2, width, width), bf16),
             pltpu.VMEM((hidden, width), bf16),
             pltpu.VMEM((hidden, width), bf16),
             like(down_post),
+            pltpu.VMEM((width, hidden), bf16),
+            pltpu.VMEM((width, hidden), bf16),
+            pltpu.VMEM((width, hidden), bf16),
+            pltpu.VMEM((width, hidden), bf16),
             like(memory_state),
             pltpu.VMEM((rows // 2, width, 2 * LANES), bf16),
             blocks(),
@@ -628,6 +690,8 @@
             pltpu.VMEM((GROUPS, total, LANES), bf16),
             pltpu.VMEM((n_kv, total, LANES), bf16),
             pltpu.VMEM((PLANE, total, LANES), bf16),
+            pltpu.VMEM((total, LANES), bf16),
+            pltpu.VMEM((total, LANES), bf16),
             pltpu.VMEM((n_kv, rows, LANES), f32),
             pltpu.VMEM((GROUPS, rows, LANES), f32),
             pltpu.VMEM((packed, LANES), f32),
@@ -638,7 +702,8 @@
             pltpu.VMEM((rows, LANES, GROUPS), f32),
             pltpu.VMEM((packed, LANES), f32),
             pltpu.VMEM((GROUPS * GROUPS, LANES), f32),
-            pltpu.VMEM((2, packed, LANES), f32),
+            pltpu.VMEM((packed, LANES), f32),
+            pltpu.VMEM((packed, LANES), f32),
             pltpu.VMEM((packed, LANES), f32),
             blocks(),
             blocks(),
@@ -648,11 +713,11 @@
             pltpu.VMEM((2, total, LANES), f32),
             pltpu.VMEM((rows, LANES), f32),
             pltpu.VMEM((rows, LANES), f32),
-            pltpu.SemaphoreType.DMA((12,)),
+            pltpu.SemaphoreType.DMA((13,)),
             pltpu.SemaphoreType.DMA((EXCHANGES,)),
             pltpu.SemaphoreType.DMA((EXCHANGES,)),
-            pltpu.SemaphoreType.DMA((8,)),
-            pltpu.SemaphoreType.DMA((8,)),
+            pltpu.SemaphoreType.DMA((9,)),
+            pltpu.SemaphoreType.DMA((9,)),
         ],
         compiler_params=pltpu.CompilerParams(
             collective_id=0, has_side_effects=True, vmem_limit_bytes=56 * 1024 * 1024

time: 52.9 us -> 53.1 us (level)
  no operation moved by 1% of the time
where the time goes in v2:
time: 53.1 us; the launch traced here: 52.9 us
  Pallas kernels  52.2 us (98%)
  between operations  0.65 us (1%)
    pallas_call x1, Pallas kernels, fused_shards(): pl.pallas_call(functools.partial(fused_layer, n_kv), out_shape=tuple((plt...  50.5 us
    pallas_call x1, Pallas kernels, fused_shards(): pl.pallas_call(store_results, out_shape=outs, in_specs=[vmem, vmem], out_...  1.72 us

profile of v2, /device:TPU:0, one launch (start us, length us, event | category | flops | bytes accessed | tf_op | source)
XLA Modules:
  0.0 52.9 jit_solution(7431556337589498583)
XLA Ops:
  0.6 50.5 %shard_map.185 = (bf16[6,1024]{1,0:T(8,128)(2,1)S(1)}, f32[6,8,128,128]{3,2,1,0:T(8,128)S(1)}) custom-call(bf16[6,1024]{1,0:T(8,128)(2,1)} %residual_ref.1, f32[1,1024]{1,0:T(1,128)} %bitcast.14, f32[16,1,128]{2,1,0:T(1,128)} %bitcast.13, f32[8,128]{1,0:T(8,128)} %bitcast.15, f32[8,128]{1,0:T(8,128)} %bitcast.16, f32[1,1024]{1,0:T(1,128)} %bitcast.17, ...), custom_call_target="tpu_custom_call" | custom-call | tf_op jit(solution)/shard_map/pallas_call | solution.py:663
  51.1 1.7 %shard_map.186 = (bf16[6,1024]{1,0:T(8,128)(2,1)}, f32[6,8,128,128]{3,2,1,0:T(8,128)}) custom-call(bf16[6,1024]{1,0:T(8,128)(2,1)S(1)} %get-tuple-element.4.layer_in, f32[6,8,128,128]{3,2,1,0:T(8,128)S(1)} %get-tuple-element.5.state_in), custom_call_target="tpu_custom_call" | custom-call | tf_op jit(solution)/shard_map/pallas_call | solution.py:745

commit v3 on v2

--- a/solution.py
+++ b/solution.py
@@ -149,9 +149,15 @@
 LANES = 128
 GROUPS = 8
 PLANE = 4
-GATHER_A, WEIGHTS, SCATTER_A, SHARE, ROWS, PROJECT, GATHER_B, SCATTER_B = range(8)
-EXCHANGES = 8
+HALVES = 2
+GATHER_A, SCATTER_A, SHARE, PROJECT, GATHER_B, SCATTER_B, WEIGHTS, ROWS = range(0, 16, HALVES)
+EXCHANGES = 16
+SQUARES, MIXED, COLUMNS = 12, 13, 14
+TP_EXCHANGES = 16
 HOLDER = 1
+WEIGHTS_EARLY = ((1, 0, 128), (2, 0, 128))
+WEIGHTS_MIDDLE = ((3, 0, 32),)
+WEIGHTS_LATE = ((3, 32, 128),)
 FLIPS = (3, 1, 2, 0)
 
 
@@ -240,6 +246,9 @@
     model = 2 * width
     total = n_kv * rows
     packed = rows * GROUPS
+    part = rows // HALVES
+    part_total = n_kv * part
+    part_packed = part * GROUPS
     planes = n_kv // PLANE
     half_planes = planes // 2
     depth_at, spot = me // PLANE, lax.rem(me, PLANE)
@@ -287,7 +296,11 @@
 
     residual = residual_ref[...].astype(f32)
     spread_rows(stream_rows, residual)
-    gather_a[me] = stream_rows[...].astype(bf16)
+    packed_parts = [
+        slice(half * part_packed, (half + 1) * part_packed) for half in range(HALVES)
+    ]
+    for half in range(HALVES):
+        gather_a[half, me] = stream_rows[packed_parts[half], :].astype(bf16)
 
     barrier = pltpu.get_barrier_semaphore()
     for peer in others():
@@ -322,120 +335,147 @@
             device_id_type=pl.DeviceIdType.MESH,
         )
 
-    def feed_forward(which, gathered, wide, gain_ref, gate, up, down):
-        wide[...] = gathered[...].astype(f32).reshape(n_kv * packed, LANES)
-        square_lanes = jnp.zeros((total, LANES), f32)
+    def gate_up(which, half, gathered, wide, gain_ref, gate, up):
+        wide[half] = gathered[half].astype(f32).reshape(part_total * GROUPS, LANES)
+        square_lanes = jnp.zeros((part_total, LANES), f32)
         for group in range(GROUPS):
-            part = wide[pl.ds(group, total, stride=GROUPS), :]
-            square_lanes += part * part
-            scaled_rows[:, lanes(group)] = (part * gain_ref[:, lanes(group)]).astype(bf16)
-        scaled = scaled_rows[...]
+            piece = wide[half, pl.ds(group, part_total, stride=GROUPS), :]
+            square_lanes += piece * piece
+            scaled_rows[half, :, lanes(group)] = (piece * gain_ref[:, lanes(group)]).astype(bf16)
+        scaled = scaled_rows[half]
         squares = jnp.sum(square_lanes, axis=1, keepdims=True)
-        squares_out[which] = jnp.broadcast_to(squares, squares_out.shape[1:])
+        squares_out[which, half] = jnp.broadcast_to(squares, squares_out.shape[2:])
+        first = 6 * which + 3 * half
+        copies = [
+            tp_copy(first, squares_out.at[which, half], squares_in.at[which, half]),
+            tp_copy(first + 1, gate_up_out.at[which, half, 0], gate_up_in.at[which, half, 0]),
+            tp_copy(first + 2, gate_up_out.at[which, half, 1], gate_up_in.at[which, half, 1]),
+        ]
         gate_part = jnp.dot(scaled, gate[...], preferred_element_type=f32)
-        gate_up_out[which, 0] = gate_part.astype(bf16)
-        copies = [
-            tp_copy(3 * which, squares_out.at[which], squares_in.at[which]),
-            tp_copy(3 * which + 1, gate_up_out.at[which, 0], gate_up_in.at[which, 0]),
-            tp_copy(3 * which + 2, gate_up_out.at[which, 1], gate_up_in.at[which, 1]),
-        ]
+        gate_up_out[which, half, 0] = gate_part.astype(bf16)
         copies[0].start()
         copies[1].start()
         up_part = jnp.dot(scaled, up[...], preferred_element_type=f32)
-        gate_up_out[which, 1] = up_part.astype(bf16)
+        gate_up_out[which, half, 1] = up_part.astype(bf16)
         copies[2].start()
+        return squares, gate_part, up_part, copies
+
+    def down_sum(which, half, parts, down):
+        squares, gate_part, up_part, copies = parts
         for copy in copies:
             copy.wait_recv()
-        inverse = lax.rsqrt((squares + squares_in[which][:, 0:1]) / model + EPSILON)
-        gate_sum = (gate_part + gate_up_in[which, 0].astype(f32)) * inverse
-        up_sum = (up_part + gate_up_in[which, 1].astype(f32)) * inverse
+        inverse = lax.rsqrt((squares + squares_in[which, half][:, 0:1]) / model + EPSILON)
+        gate_sum = (gate_part + gate_up_in[which, half, 0].astype(f32)) * inverse
+        up_sum = (up_part + gate_up_in[which, half, 1].astype(f32)) * inverse
         hidden = (gate_sum / (1.0 + jnp.exp(-gate_sum)) * up_sum).astype(bf16)
-        return jnp.dot(hidden, down[...], preferred_element_type=f32), copies
+        return jnp.dot(hidden, down[...], preferred_element_type=f32)
 
     def gather_start(exchange, gathered):
-        for peer in others():
-            remote(exchange, gathered.at[me], gathered.at[me], kv=peer).start()
+        for half in range(HALVES):
+            block = gathered.at[half, me]
+            for peer in others():
+                remote(exchange + half, block, block, kv=peer).start()
 
     def turn(target, source):
         for group in range(GROUPS):
             target[lanes(group), :] = source[:, lanes(group)].T
 
-    def but_one(ref):
-        return ref.at[pl.ds(0, n_kv - 1)]
+    def but_one(ref, half):
+        return ref.at[half, pl.ds(0, n_kv - 1)]
 
     gather_start(GATHER_A, gather_a)
     for copy in loads[0:4]:
         copy.wait()
-    for flip in FLIPS[:-1]:
-        peer_spot = flipped(flip)
-        remote(
-            WEIGHTS,
-            own_weights.at[peer_spot],
-            plane_weights.at[spot],
-            kv=depth_at * PLANE + peer_spot,
-        ).start()
+    def send_weights(*flips):
+        for flip, low, high in flips:
+            peer_spot = flipped(flip)
+            span = pl.ds(low, high - low)
+            remote(
+                WEIGHTS,
+                own_weights.at[peer_spot, span],
+                plane_weights.at[spot, span],
+                kv=depth_at * PLANE + peer_spot,
+            ).start()
+
+    send_weights(*WEIGHTS_EARLY)
     plane_weights[spot] = own_weights[spot]
     mixed_rows[packed:, :] = jnp.zeros((mixed_rows.shape[0] - packed, LANES), f32)
     for copy in loads[4:7]:
         copy.wait()
     turn(gate_pre_t, gate_pre)
     turn(up_pre_t, up_pre)
-    all_of(GATHER_A, but_one(gather_a)).wait_recv()
-    branch_a, copies_a = feed_forward(
-        0, gather_a, wide_a, gain_pre_ref, gate_pre_t, up_pre_t, down_pre
-    )
-    for group in range(GROUPS):
-        columns_out[group] = branch_a[:, lanes(group)].astype(bf16)
-    shared_copy = tp_copy(8, shared_out, shared_in)
+    parts_a = []
+    for half in range(HALVES):
+        all_of(GATHER_A + half, but_one(gather_a, half)).wait_recv()
+        if half == HALVES - 1:
+            send_weights(*WEIGHTS_MIDDLE)
+        parts_a.append(
+            gate_up(0, half, gather_a, wide_a, gain_pre_ref, gate_pre_t, up_pre_t)
+        )
+    shared_copies = [
+        tp_copy(COLUMNS + half, shared_out.at[half], shared_in.at[half]) for half in range(HALVES)
+    ]
 
     @pl.when(owner_core == core)
     def _():
-        shared_out[...] = wide_a[pl.ds(slot, total, stride=GROUPS), :].astype(bf16)
+        for half in range(HALVES):
+            shared_out[half] = wide_a[half, pl.ds(slot, part_total, stride=GROUPS), :].astype(bf16)
 
         @pl.when(jnp.logical_not(holder))
         def _():
-            shared_copy.start()
-
-    for flip in FLIPS:
-        for step in range(half_planes - 1, -1, -1):
-            plane = core * half_planes + lax.rem(depth_at + step, half_planes)
-            peer = plane * PLANE + flipped(flip)
-            copy = remote(
-                SCATTER_A,
-                columns_out.at[lax.rem(peer, GROUPS)],
-                columns_landed.at[me],
-                kv=peer,
-                tp=HOLDER,
-            )
-            if step or flip:
+            for copy in shared_copies:
                 copy.start()
-            else:
-                pl.when(jnp.logical_not(owns))(copy.start)
+
+    for half in range(HALVES):
+        branch_a = down_sum(0, half, parts_a[half], down_pre)
+        for group in range(GROUPS):
+            columns_out[half, group] = branch_a[:, lanes(group)].astype(bf16)
+        for flip in FLIPS:
+            for step in range(half_planes - 1, -1, -1):
+                plane = core * half_planes + lax.rem(depth_at + step, half_planes)
+                peer = plane * PLANE + flipped(flip)
+                copy = remote(
+                    SCATTER_A + half,
+                    columns_out.at[half, lax.rem(peer, GROUPS)],
+                    columns_landed.at[half, me],
+                    kv=peer,
+                    tp=HOLDER,
+                )
+                if step or flip:
+                    copy.start()
+                else:
+                    pl.when(jnp.logical_not(owns))(copy.start)
+
+    send_weights(*WEIGHTS_LATE)
 
     @pl.when(holder)
     def _():
-        @pl.when(owns)
-        def _():
-            columns_landed[me] = columns_out[slot]
-            all_of(SCATTER_A, but_one(columns_landed)).wait_recv()
-            shared_in[...] = shared_out[...]
-
-        @pl.when(jnp.logical_not(owns))
-        def _():
-            all_of(SCATTER_A, columns_landed).wait_recv()
-            shared_copy.wait_recv()
-
-        branch = jnp.sum(columns_landed[...].astype(f32), axis=0)
-        stream = (shared_in[...].astype(f32) + 0.5 * branch).astype(bf16).astype(f32)
-        columns_in[spot] = (stream * gain_mix_ref[me]).astype(bf16)
-        block = columns_in.at[spot]
-        for flip in FLIPS:
-            peer = depth_at * PLANE + flipped(flip)
-            remote(SHARE, block, block, kv=peer, tp=1 - core).start()
-            if flip:
-                remote(SHARE, block, block, kv=peer, tp=core).start()
-        for owner in range(n_kv):
-            rows_out[owner] = stream[owner * rows : (owner + 1) * rows, :]
+        for half in range(HALVES):
+
+            @pl.when(owns)
+            def _():
+                columns_landed[half, me] = columns_out[half, slot]
+                shared_in[half] = shared_out[half]
+                all_of(SCATTER_A + half, but_one(columns_landed, half)).wait_recv()
+
+            @pl.when(jnp.logical_not(owns))
+            def _():
+                shared_copies[half].wait_recv()
+                all_of(SCATTER_A + half, columns_landed.at[half]).wait_recv()
+
+            branch = jnp.sum(columns_landed[half].astype(f32), axis=0)
+            stream = (shared_in[half].astype(f32) + 0.5 * branch).astype(bf16).astype(f32)
+            columns_in[half, spot] = (stream * gain_mix_ref[me]).astype(bf16)
+            block = columns_in.at[half, spot]
+            for flip in FLIPS:
+                peer = depth_at * PLANE + flipped(flip)
+                remote(SHARE + half, block, block, kv=peer, tp=1 - core).start()
+                if flip:
+                    remote(SHARE + half, block, block, kv=peer, tp=core).start()
+            for owner in range(n_kv):
+                rows_out[owner, half * part : (half + 1) * part, :] = stream[
+                    owner * part : (owner + 1) * part, :
+                ]
         for peer in others():
             remote(ROWS, rows_out.at[peer], rows_in.at[slot], kv=peer, tp=owner_core).start()
 
@@ -447,24 +487,29 @@
         def _():
             remote(ROWS, rows_out.at[me], rows_in.at[slot], tp=1 - core).start()
 
-        all_of(SHARE, columns_in.at[pl.ds(0, PLANE - 1)]).wait_recv()
-
-    @pl.when(jnp.logical_not(holder))
-    def _():
-        all_of(SHARE, columns_in).wait_recv()
-
-    all_of(WEIGHTS, plane_weights.at[pl.ds(0, PLANE - 1)]).wait_recv()
-    columns = jnp.concatenate([columns_in[part] for part in range(PLANE)], axis=1)
-    product = jnp.dot(
-        columns,
-        plane_weights[...].reshape(PLANE * LANES, width),
-        preferred_element_type=f32,
-    )
-    spread_rows(spread, product)
-    proj_out[...] = spread[...].astype(bf16).reshape(n_kv, packed, LANES)
-    for peer in others():
-        remote(PROJECT, proj_out.at[peer], proj_in.at[me], kv=peer).start()
-    proj_in[me] = proj_out[me]
+    for half in range(HALVES):
+
+        @pl.when(holder)
+        def _():
+            all_of(SHARE + half, columns_in.at[half, pl.ds(0, PLANE - 1)]).wait_recv()
+
+        @pl.when(jnp.logical_not(holder))
+        def _():
+            all_of(SHARE + half, columns_in.at[half]).wait_recv()
+
+        if half == 0:
+            all_of(WEIGHTS, plane_weights.at[pl.ds(0, PLANE - 1)]).wait_recv()
+        columns = jnp.concatenate([columns_in[half, place] for place in range(PLANE)], axis=1)
+        product = jnp.dot(
+            columns,
+            plane_weights[...].reshape(PLANE * LANES, width),
+            preferred_element_type=f32,
+        )
+        spread_rows(spread.at[half], product)
+        proj_out[half] = spread[half].astype(bf16).reshape(n_kv, part_packed, LANES)
+        for peer in others():
+            remote(PROJECT + half, proj_out.at[half, peer], proj_in.at[half, me], kv=peer).start()
+        proj_in[half, me] = proj_out[half, me]
 
     @pl.when(owns)
     def _():
@@ -479,7 +524,7 @@
     stream = stream_rows[...].reshape(rows, GROUPS, LANES)
     row_squares = jnp.sum(stream * stream, axis=1)
     row_squares_out[...] = row_squares
-    square_copy = tp_copy(6, row_squares_out, row_squares_in)
+    square_copy = tp_copy(SQUARES, row_squares_out, row_squares_in)
     square_copy.start()
     loads[7].wait()
     for row in range(rows):
@@ -500,11 +545,15 @@
         )
     loads[8].wait()
     loads[9].wait()
-    all_of(PROJECT, but_one(proj_in)).wait_recv()
+    for half in range(HALVES):
+        all_of(PROJECT + half, but_one(proj_in, half)).wait_recv()
 
     def projected(index):
-        parts = [proj_in[plane * PLANE + index].astype(f32) for plane in range(planes)]
-        return sum(parts[1:], parts[0]) * inverse_rows[...]
+        sums = []
+        for half in range(HALVES):
+            terms = [proj_in[half, plane * PLANE + index].astype(f32) for plane in range(planes)]
+            sums.append(sum(terms[1:], terms[0]))
+        return jnp.concatenate(sums, axis=0) * inverse_rows[...]
 
     floor_rate = jnp.concatenate([lower_ref[...]] * rows, axis=0)
     forget_pre = projected(0)
@@ -545,7 +594,7 @@
     ).astype(bf16)
     away = jnp.dot(mixed_heads, out_weight[1 - core], preferred_element_type=f32)
     spread_rows(mixed_out, away[0:rows])
-    mixed_copy = tp_copy(7, mixed_out, mixed_in)
+    mixed_copy = tp_copy(MIXED, mixed_out, mixed_in)
     mixed_copy.start()
     home = jnp.dot(mixed_heads, out_weight[core], preferred_element_type=f32)
     spread_rows(mixed_own, home[0:rows])
@@ -555,7 +604,8 @@
         inject_t[row] = inject[span].T
     mixed_copy.wait_recv()
     stream_b = (stream_rows[...] + (mixed_own[...] + mixed_in[...])).astype(bf16)
-    gather_b[me] = stream_b
+    for half in range(HALVES):
+        gather_b[half, me] = stream_b[packed_parts[half], :]
     gather_start(GATHER_B, gather_b)
 
     def update(row, carry):
@@ -571,34 +621,46 @@
 
     lax.fori_loop(0, rows, update, 0)
     loads[12].wait()
-    all_of(GATHER_B, but_one(gather_b)).wait_recv()
-    branch_b, copies_b = feed_forward(
-        1, gather_b, wide_b, gain_post_ref, gate_post_t, up_post_t, down_post
-    )
-    spread_rows(spread, branch_b)
-    partial_b[...] = spread[...].astype(bf16).reshape(n_kv, packed, LANES)
-    for peer in others():
-        remote(SCATTER_B, partial_b.at[peer], landed_b.at[me], kv=peer).start()
-    landed_b[me] = partial_b[me]
-    for copy in copies_a + copies_b + [square_copy, mixed_copy]:
+    parts_b = []
+    for half in range(HALVES):
+        all_of(GATHER_B + half, but_one(gather_b, half)).wait_recv()
+        parts_b.append(
+            gate_up(1, half, gather_b, wide_b, gain_post_ref, gate_post_t, up_post_t)
+        )
+    for half in range(HALVES):
+        branch_b = down_sum(1, half, parts_b[half], down_post)
+        spread_rows(spread.at[half], branch_b)
+        partial_b[half] = spread[half].astype(bf16).reshape(n_kv, part_packed, LANES)
+        for peer in others():
+            remote(
+                SCATTER_B + half, partial_b.at[half, peer], landed_b.at[half, me], kv=peer
+            ).start()
+        landed_b[half, me] = partial_b[half, me]
+    for copy in parts_a[0][3] + parts_a[1][3] + parts_b[0][3] + parts_b[1][3]:
         copy.wait_send()
-    all_of(GATHER_A, but_one(gather_a)).wait_send()
+    square_copy.wait_send()
+    mixed_copy.wait_send()
     all_of(WEIGHTS, plane_weights.at[pl.ds(0, PLANE - 1)]).wait_send()
-    all_of(PROJECT, but_one(proj_out)).wait_send()
-    all_of(GATHER_B, but_one(gather_b)).wait_send()
+    for half in range(HALVES):
+        all_of(GATHER_A + half, but_one(gather_a, half)).wait_send()
+        all_of(PROJECT + half, but_one(proj_out, half)).wait_send()
+        all_of(GATHER_B + half, but_one(gather_b, half)).wait_send()
 
     @pl.when(holder)
     def _():
-        all_of(SHARE, columns_landed.at[pl.ds(0, 2 * PLANE - 1)]).wait_send()
+        for half in range(HALVES):
+            all_of(SHARE + half, columns_landed.at[half, pl.ds(0, 2 * PLANE - 1)]).wait_send()
 
     @pl.when(owns)
     def _():
-        all_of(SCATTER_A, columns_out.at[pl.ds(0, GROUPS - 1)]).wait_send()
-        all_of(ROWS, but_one(rows_out)).wait_send()
+        for half in range(HALVES):
+            all_of(SCATTER_A + half, columns_out.at[half, pl.ds(0, GROUPS - 1)]).wait_send()
+        all_of(ROWS, rows_out.at[pl.ds(0, n_kv - 1)]).wait_send()
 
     @pl.when(jnp.logical_not(owns))
     def _():
-        all_of(SCATTER_A, columns_out).wait_send()
+        for half in range(HALVES):
+            all_of(SCATTER_A + half, columns_out.at[half]).wait_send()
 
         @pl.when(holder)
         def _():
@@ -606,14 +668,17 @@
 
     @pl.when(jnp.logical_and(owner_core == core, jnp.logical_not(holder)))
     def _():
-        shared_copy.wait_send()
-
-    all_of(SCATTER_B, but_one(landed_b)).wait_recv()
-    branch = jnp.sum(landed_b[...].astype(f32), axis=0)
-    spread[0:packed, :] = gather_b[me].astype(f32) + 0.5 * branch
+        for copy in shared_copies:
+            copy.wait_send()
+
+    for half in range(HALVES):
+        all_of(SCATTER_B + half, but_one(landed_b, half)).wait_recv()
+        branch = jnp.sum(landed_b[half].astype(f32), axis=0)
+        mixed_rows[packed_parts[half], :] = gather_b[half, me].astype(f32) + 0.5 * branch
     for group in range(GROUPS):
-        layer_ref[:, lanes(group)] = spread[pl.ds(group, rows, stride=GROUPS), :].astype(bf16)
-    all_of(SCATTER_B, but_one(partial_b)).wait_send()
+        layer_ref[:, lanes(group)] = mixed_rows[pl.ds(group, rows, stride=GROUPS), :].astype(bf16)
+    for half in range(HALVES):
+        all_of(SCATTER_B + half, but_one(partial_b, half)).wait_send()
 
 
 def store_results(layer_in, state_in, layer_out, state_out, sem):
@@ -655,7 +720,9 @@
     vmem = pl.BlockSpec(memory_space=pltpu.VMEM)
     hbm = pl.BlockSpec(memory_space=pltpu.HBM)
     like = lambda array: pltpu.VMEM(array.shape, array.dtype)
-    blocks = lambda: pltpu.VMEM((n_kv, packed, LANES), bf16)
+    part_total = total // HALVES
+    blocks = lambda: pltpu.VMEM((HALVES, n_kv, packed // HALVES, LANES), bf16)
+    halves = lambda *shape: pltpu.VMEM((HALVES,) + shape, bf16)
     outs = (
         jax.ShapeDtypeStruct(residual_in.shape, residual_in.dtype),
         jax.ShapeDtypeStruct(memory_state.shape, memory_state.dtype),
@@ -683,15 +750,15 @@
             pltpu.VMEM((rows // 2, width, 2 * LANES), bf16),
             blocks(),
             blocks(),
-            pltpu.VMEM((n_kv * packed, LANES), f32),
-            pltpu.VMEM((n_kv * packed, LANES), f32),
-            pltpu.VMEM((n_kv * packed, LANES), f32),
-            pltpu.VMEM((total, width), bf16),
-            pltpu.VMEM((GROUPS, total, LANES), bf16),
-            pltpu.VMEM((n_kv, total, LANES), bf16),
-            pltpu.VMEM((PLANE, total, LANES), bf16),
-            pltpu.VMEM((total, LANES), bf16),
-            pltpu.VMEM((total, LANES), bf16),
+            pltpu.VMEM((HALVES, part_total * GROUPS, LANES), f32),
+            pltpu.VMEM((HALVES, part_total * GROUPS, LANES), f32),
+            pltpu.VMEM((HALVES, part_total * GROUPS, LANES), f32),
+            halves(part_total, width),
+            halves(GROUPS, part_total, LANES),
+            halves(n_kv, part_total, LANES),
+            halves(PLANE, part_total, LANES),
+            halves(part_total, LANES),
+            halves(part_total, LANES),
             pltpu.VMEM((n_kv, rows, LANES), f32),
             pltpu.VMEM((GROUPS, rows, LANES), f32),
             pltpu.VMEM((packed, LANES), f32),
@@ -707,17 +774,17 @@
             pltpu.VMEM((packed, LANES), f32),
             blocks(),
             blocks(),
-            pltpu.VMEM((2, 2, total, hidden), bf16),
-            pltpu.VMEM((2, 2, total, hidden), bf16),
-            pltpu.VMEM((2, total, LANES), f32),
-            pltpu.VMEM((2, total, LANES), f32),
+            pltpu.VMEM((2, HALVES, 2, part_total, hidden), bf16),
+            pltpu.VMEM((2, HALVES, 2, part_total, hidden), bf16),
+            pltpu.VMEM((2, HALVES, part_total, LANES), f32),
+            pltpu.VMEM((2, HALVES, part_total, LANES), f32),
             pltpu.VMEM((rows, LANES), f32),
             pltpu.VMEM((rows, LANES), f32),
             pltpu.SemaphoreType.DMA((13,)),
             pltpu.SemaphoreType.DMA((EXCHANGES,)),
             pltpu.SemaphoreType.DMA((EXCHANGES,)),
-            pltpu.SemaphoreType.DMA((9,)),
-            pltpu.SemaphoreType.DMA((9,)),
+            pltpu.SemaphoreType.DMA((TP_EXCHANGES,)),
+            pltpu.SemaphoreType.DMA((TP_EXCHANGES,)),
         ],
         compiler_params=pltpu.CompilerParams(
             collective_id=0, has_side_effects=True, vmem_limit_bytes=56 * 1024 * 1024

time: 53.1 us -> 50.7 us (0.955)
  Pallas kernels: 52.2 us -> 49.9 us
    pallas_call x1, Pallas kernels: 50.5 us -> 48.1 us  [fused_shards(): pl.pallas_call(functools.partial(fused_layer, n_kv), out_shape=tuple((plt...]
where the time goes in v3:
time: 50.7 us; the launch traced here: 50.5 us
  Pallas kernels  49.9 us (98%)
  between operations  0.65 us (1%)
    pallas_call x1, Pallas kernels, fused_shards(): pl.pallas_call(functools.partial(fused_layer, n_kv), out_shape=tuple((plt...  48.1 us
    pallas_call x1, Pallas kernels, fused_shards(): pl.pallas_call(store_results, out_shape=outs, in_specs=[vmem, vmem], out_...  1.72 us

profile of v3, /device:TPU:0, one launch (start us, length us, event | category | flops | bytes accessed | tf_op | source)
XLA Modules:
  0.0 50.5 jit_solution(5576059687182270847)
XLA Ops:
  0.6 48.1 %shard_map.185 = (bf16[6,1024]{1,0:T(8,128)(2,1)S(1)}, f32[6,8,128,128]{3,2,1,0:T(8,128)S(1)}) custom-call(bf16[6,1024]{1,0:T(8,128)(2,1)} %residual_ref.1, f32[1,1024]{1,0:T(1,128)} %bitcast.14, f32[16,1,128]{2,1,0:T(1,128)} %bitcast.13, f32[8,128]{1,0:T(8,128)} %bitcast.15, f32[8,128]{1,0:T(8,128)} %bitcast.16, f32[1,1024]{1,0:T(1,128)} %bitcast.17, ...), custom_call_target="tpu_custom_call" | custom-call | tf_op jit(solution)/shard_map/pallas_call | solution.py:730
  48.8 1.7 %shard_map.186 = (bf16[6,1024]{1,0:T(8,128)(2,1)}, f32[6,8,128,128]{3,2,1,0:T(8,128)}) custom-call(bf16[6,1024]{1,0:T(8,128)(2,1)S(1)} %get-tuple-element.4.layer_in, f32[6,8,128,128]{3,2,1,0:T(8,128)S(1)} %get-tuple-element.5.state_in), custom_call_target="tpu_custom_call" | custom-call | tf_op jit(solution)/shard_map/pallas_call | solution.py:812

commit v4 on v3

--- a/solution.py
+++ b/solution.py
@@ -151,13 +151,14 @@
 PLANE = 4
 HALVES = 2
 GATHER_A, SCATTER_A, SHARE, PROJECT, GATHER_B, SCATTER_B, WEIGHTS, ROWS = range(0, 16, HALVES)
-EXCHANGES = 16
+EXCHANGES = 17
+RELAY = 16
 SQUARES, MIXED, COLUMNS = 12, 13, 14
 TP_EXCHANGES = 16
 HOLDER = 1
-WEIGHTS_EARLY = ((1, 0, 128), (2, 0, 128))
-WEIGHTS_MIDDLE = ((3, 0, 32),)
-WEIGHTS_LATE = ((3, 32, 128),)
+EARLY_ROWS = LANES // 4
+WEIGHTS_EARLY = ((3, 0, LANES), (1, 0, EARLY_ROWS), (2, 0, EARLY_ROWS))
+WEIGHTS_LATE = ((1, EARLY_ROWS, LANES), (2, EARLY_ROWS, LANES))
 FLIPS = (3, 1, 2, 0)
 
 
@@ -192,6 +193,7 @@
     down_pre,
     own_weights,
     plane_weights,
+    relayed,
     out_weight,
     gate_post,
     up_post,
@@ -386,18 +388,30 @@
     gather_start(GATHER_A, gather_a)
     for copy in loads[0:4]:
         copy.wait()
-    def send_weights(*flips):
+    def send_weights(source, target_core, flips):
         for flip, low, high in flips:
             peer_spot = flipped(flip)
             span = pl.ds(low, high - low)
             remote(
-                WEIGHTS,
-                own_weights.at[peer_spot, span],
+                WEIGHTS + target_core,
+                source.at[peer_spot, span],
                 plane_weights.at[spot, span],
                 kv=depth_at * PLANE + peer_spot,
+                tp=target_core,
             ).start()
 
-    send_weights(*WEIGHTS_EARLY)
+    @pl.when(holder)
+    def _():
+        for flip in FLIPS[1:3] + FLIPS[0:1]:
+            block = flipped(flip)
+            remote(RELAY, own_weights.at[block], relayed.at[block], tp=1 - core).start()
+
+    @pl.when(jnp.logical_not(holder))
+    def _():
+        send_weights(own_weights, 1 - HOLDER, WEIGHTS_EARLY)
+        all_of(RELAY, relayed.at[pl.ds(0, PLANE - 1)]).wait_recv()
+        send_weights(relayed, HOLDER, WEIGHTS_EARLY)
+
     plane_weights[spot] = own_weights[spot]
     mixed_rows[packed:, :] = jnp.zeros((mixed_rows.shape[0] - packed, LANES), f32)
     for copy in loads[4:7]:
@@ -407,8 +421,6 @@
     parts_a = []
     for half in range(HALVES):
         all_of(GATHER_A + half, but_one(gather_a, half)).wait_recv()
-        if half == HALVES - 1:
-            send_weights(*WEIGHTS_MIDDLE)
         parts_a.append(
             gate_up(0, half, gather_a, wide_a, gain_pre_ref, gate_pre_t, up_pre_t)
         )
@@ -446,7 +458,10 @@
                 else:
                     pl.when(jnp.logical_not(owns))(copy.start)
 
-    send_weights(*WEIGHTS_LATE)
+    @pl.when(jnp.logical_not(holder))
+    def _():
+        send_weights(own_weights, 1 - HOLDER, WEIGHTS_LATE)
+        send_weights(relayed, HOLDER, WEIGHTS_LATE)
 
     @pl.when(holder)
     def _():
@@ -498,7 +513,7 @@
             all_of(SHARE + half, columns_in.at[half]).wait_recv()
 
         if half == 0:
-            all_of(WEIGHTS, plane_weights.at[pl.ds(0, PLANE - 1)]).wait_recv()
+            all_of(WEIGHTS + core, plane_weights.at[pl.ds(0, PLANE - 1)]).wait_recv()
         columns = jnp.concatenate([columns_in[half, place] for place in range(PLANE)], axis=1)
         product = jnp.dot(
             columns,
@@ -640,14 +655,19 @@
         copy.wait_send()
     square_copy.wait_send()
     mixed_copy.wait_send()
-    all_of(WEIGHTS, plane_weights.at[pl.ds(0, PLANE - 1)]).wait_send()
     for half in range(HALVES):
         all_of(GATHER_A + half, but_one(gather_a, half)).wait_send()
         all_of(PROJECT + half, but_one(proj_out, half)).wait_send()
         all_of(GATHER_B + half, but_one(gather_b, half)).wait_send()
 
+    @pl.when(jnp.logical_not(holder))
+    def _():
+        for target_core in range(2):
+            all_of(WEIGHTS + target_core, plane_weights.at[pl.ds(0, PLANE - 1)]).wait_send()
+
     @pl.when(holder)
     def _():
+        all_of(RELAY, relayed.at[pl.ds(0, PLANE - 1)]).wait_send()
         for half in range(HALVES):
             all_of(SHARE + half, columns_landed.at[half, pl.ds(0, 2 * PLANE - 1)]).wait_send()
 
@@ -736,6 +756,7 @@
             pltpu.VMEM((hidden, width), bf16),
             pltpu.VMEM((hidden, width), bf16),
             like(down_pre),
+            pltpu.VMEM((PLANE,) + query_weight.shape, bf16),
             pltpu.VMEM((PLANE,) + query_weight.shape, bf16),
             pltpu.VMEM((PLANE,) + query_weight.shape, bf16),
             pltpu.VMEM((2, width, width), bf16),

time: 50.7 us -> 49.1 us (0.968)
  Pallas kernels: 49.9 us -> 48.2 us
    pallas_call x1, Pallas kernels: 48.1 us -> 46.5 us  [fused_shards(): pl.pallas_call(functools.partial(fused_layer, n_kv), out_shape=tuple((plt...]
where the time goes in v4:
time: 49.1 us; the launch traced here: 48.9 us
  Pallas kernels  48.2 us (98%)
  between operations  0.65 us (1%)
    pallas_call x1, Pallas kernels, fused_shards(): pl.pallas_call(functools.partial(fused_layer, n_kv), out_shape=tuple((plt...  46.5 us
    pallas_call x1, Pallas kernels, fused_shards(): pl.pallas_call(store_results, out_shape=outs, in_specs=[vmem, vmem], out_...  1.72 us

profile of v4, /device:TPU:0, one launch (start us, length us, event | category | flops | bytes accessed | tf_op | source)
XLA Modules:
  0.0 48.9 jit_solution(14830843612182209369)
XLA Ops:
  0.6 46.5 %shard_map.185 = (bf16[6,1024]{1,0:T(8,128)(2,1)S(1)}, f32[6,8,128,128]{3,2,1,0:T(8,128)S(1)}) custom-call(bf16[6,1024]{1,0:T(8,128)(2,1)} %residual_ref.1, f32[1,1024]{1,0:T(1,128)} %bitcast.14, f32[16,1,128]{2,1,0:T(1,128)} %bitcast.13, f32[8,128]{1,0:T(8,128)} %bitcast.15, f32[8,128]{1,0:T(8,128)} %bitcast.16, f32[1,1024]{1,0:T(1,128)} %bitcast.17, ...), custom_call_target="tpu_custom_call" | custom-call | tf_op jit(solution)/shard_map/pallas_call | solution.py:750
  47.2 1.7 %shard_map.186 = (bf16[6,1024]{1,0:T(8,128)(2,1)}, f32[6,8,128,128]{3,2,1,0:T(8,128)}) custom-call(bf16[6,1024]{1,0:T(8,128)(2,1)S(1)} %get-tuple-element.4.layer_in, f32[6,8,128,128]{3,2,1,0:T(8,128)S(1)} %get-tuple-element.5.state_in), custom_call_target="tpu_custom_call" | custom-call | tf_op jit(solution)/shard_map/pallas_call | solution.py:833

commit v5 on v4

--- a/solution.py
+++ b/solution.py
@@ -560,47 +560,51 @@
         )
     loads[8].wait()
     loads[9].wait()
+    floor_rate = jnp.concatenate([lower_ref[...]] * part, axis=0)
+    head_index = lax.broadcasted_iota(jnp.int32, (GROUPS, LANES), 0)
+    keeps, injects, weights, directs, outgates, read = [], [], [], [], [], []
+
+    def diagonal(row):
+        span = slice(row % part * GROUPS, (row % part + 1) * GROUPS)
+        heads = weights[row // part][span]
+        return jnp.concatenate(
+            [jnp.where(head_index == head, heads, 0.0) for head in range(GROUPS)], axis=1
+        )
+
+    def read_pairs(ready):
+        while len(read) + 1 < ready:
+            row = len(read)
+            both = jnp.dot(
+                jnp.concatenate([diagonal(row), diagonal(row + 1)], axis=0).astype(bf16),
+                state_half[row // 2],
+                preferred_element_type=f32,
+            )
+            read.append(both[0:GROUPS, lanes(0)])
+            read.append(both[GROUPS : 2 * GROUPS, lanes(1)])
+
     for half in range(HALVES):
         all_of(PROJECT + half, but_one(proj_in, half)).wait_recv()
 
-    def projected(index):
-        sums = []
-        for half in range(HALVES):
+        def projected(index):
             terms = [proj_in[half, plane * PLANE + index].astype(f32) for plane in range(planes)]
-            sums.append(sum(terms[1:], terms[0]))
-        return jnp.concatenate(sums, axis=0) * inverse_rows[...]
-
-    floor_rate = jnp.concatenate([lower_ref[...]] * rows, axis=0)
-    forget_pre = projected(0)
-    keep = floor_rate + (1.0 - floor_rate) / (1.0 + jnp.exp(-forget_pre))
-    inject = (1.0 - floor_rate) / (1.0 + jnp.exp(forget_pre))
-    query_pre = projected(2)
-    query = query_pre / (1.0 + jnp.exp(-query_pre))
-    value = projected(1)
-    value_rows[...] = value
-    weighted = query * keep
-    direct = jnp.sum(query * inject, axis=1, keepdims=True) * value
-    head_index = lax.broadcasted_iota(jnp.int32, (GROUPS, LANES), 0)
-    read = []
-    for pair in range(rows // 2):
-        diagonal = []
-        for row in (2 * pair, 2 * pair + 1):
-            heads = weighted[row * GROUPS : (row + 1) * GROUPS, :]
-            diagonal.append(
-                jnp.concatenate(
-                    [jnp.where(head_index == head, heads, 0.0) for head in range(GROUPS)], axis=1
-                )
-            )
-        both = jnp.dot(
-            jnp.concatenate(diagonal, axis=0).astype(bf16),
-            state_half[pair],
-            preferred_element_type=f32,
-        )
-        read.append(both[0:GROUPS, lanes(0)])
-        read.append(both[GROUPS : 2 * GROUPS, lanes(1)])
-    readout = jnp.concatenate(read, axis=0) + direct
-    outgate_pre = projected(3)
-    outgate = outgate_pre / (1.0 + jnp.exp(-outgate_pre))
+            return sum(terms[1:], terms[0]) * inverse_rows[packed_parts[half], :]
+
+        forget_pre = projected(0)
+        keeps.append(floor_rate + (1.0 - floor_rate) / (1.0 + jnp.exp(-forget_pre)))
+        injects.append((1.0 - floor_rate) / (1.0 + jnp.exp(forget_pre)))
+        query_pre = projected(2)
+        query = query_pre / (1.0 + jnp.exp(-query_pre))
+        value = projected(1)
+        value_rows[packed_parts[half], :] = value
+        weights.append(query * keeps[half])
+        directs.append(jnp.sum(query * injects[half], axis=1, keepdims=True) * value)
+        outgate_pre = projected(3)
+        outgates.append(outgate_pre / (1.0 + jnp.exp(-outgate_pre)))
+        read_pairs((half + 1) * part)
+    keep = jnp.concatenate(keeps, axis=0)
+    inject = jnp.concatenate(injects, axis=0)
+    outgate = jnp.concatenate(outgates, axis=0)
+    readout = jnp.concatenate(read, axis=0) + jnp.concatenate(directs, axis=0)
     scale = lax.rsqrt(jnp.mean(readout * readout, axis=1, keepdims=True) + EPSILON)
     head_gain = jnp.concatenate([head_gain_ref[...]] * rows, axis=0)
     mixed_rows[0:packed, :] = readout * scale * head_gain * outgate

time: 49.1 us -> 49 us (level)
  no operation moved by 1% of the time
where the time goes in v5:
time: 49 us; the launch traced here: 48.8 us
  Pallas kernels  48.2 us (98%)
  between operations  0.65 us (1%)
    pallas_call x1, Pallas kernels, fused_shards(): pl.pallas_call(functools.partial(fused_layer, n_kv), out_shape=tuple((plt...  46.4 us
    pallas_call x1, Pallas kernels, fused_shards(): pl.pallas_call(store_results, out_shape=outs, in_specs=[vmem, vmem], out_...  1.72 us

profile of v5, /device:TPU:0, one launch (start us, length us, event | category | flops | bytes accessed | tf_op | source)
XLA Modules:
  0.0 48.8 jit_solution(6002088733712980934)
XLA Ops:
  0.6 46.4 %shard_map.185 = (bf16[6,1024]{1,0:T(8,128)(2,1)S(1)}, f32[6,8,128,128]{3,2,1,0:T(8,128)S(1)}) custom-call(bf16[6,1024]{1,0:T(8,128)(2,1)} %residual_ref.1, f32[1,1024]{1,0:T(1,128)} %bitcast.14, f32[16,1,128]{2,1,0:T(1,128)} %bitcast.13, f32[8,128]{1,0:T(8,128)} %bitcast.15, f32[8,128]{1,0:T(8,128)} %bitcast.16, f32[1,1024]{1,0:T(1,128)} %bitcast.17, ...), custom_call_target="tpu_custom_call" | custom-call | tf_op jit(solution)/shard_map/pallas_call | solution.py:754
  47.1 1.7 %shard_map.186 = (bf16[6,1024]{1,0:T(8,128)(2,1)}, f32[6,8,128,128]{3,2,1,0:T(8,128)}) custom-call(bf16[6,1024]{1,0:T(8,128)(2,1)S(1)} %get-tuple-element.4.layer_in, f32[6,8,128,128]{3,2,1,0:T(8,128)S(1)} %get-tuple-element.5.state_in), custom_call_target="tpu_custom_call" | custom-call | tf_op jit(solution)/shard_map/pallas_call | solution.py:837
